TPU v7x, 32 devices: a whole 2x2x4 slice. The times are simulated.
32 devices in a mesh: grp: 2 (over x), ep: 8 (over z, y), tp: 2 (over core).
Axes of the slice: x: 2, y: 2, z: 4, core: 2. Of those that a mesh axis runs over, the one named last changes fastest.
Arguments:
- tokens: bfloat16 [8192, 2048], P(('grp', 'ep', 'tp')), parts along dimension 0, may hold values from -6 to 6
- norm_gain: float32 [2048], replicated, may hold values from 0.1 to 1.9
- route_ids: int32 [8192, 2], P(('grp', 'ep', 'tp')), parts along dimension 0, may hold values from 0 to 7, as said below
- route_weights: float32 [8192, 2], P(('grp', 'ep', 'tp')), parts along dimension 0, may hold values from 0.1 to 1
- w_gate: bfloat16 [8, 2048, 512], P('ep', None, 'tp'), may hold values from -0.125 to 0.125
- w_up: bfloat16 [8, 2048, 512], P('ep', None, 'tp'), may hold values from -0.125 to 0.125
- w_down: bfloat16 [8, 512, 2048], P('ep', 'tp'), may hold values from -0.25 to 0.25
Outputs:
- mixed: bfloat16 [8192, 2048], P(('grp', 'ep', 'tp')), parts along dimension 0
There are 2 independent parts, one for each index of `grp`. A program takes and returns all parts, laid end to end along the dimension named above; an argument that names none is the same for every part. Nothing has to cross between parts.
Inputs may be any that keep to these rules, and one draw needn't show every extreme that they name: `route_ids`: the 2 experts of a token are different and lie in one group of 2 consecutive experts. Among the tokens of one device (aligned blocks of 256 tokens) no expert is named more than 128 times, and in every such block some expert is named exactly 128 times.
All inputs are finite; a program needn't handle non-finite values.
Results may differ from a plain program's by a relative error of at most 0.007.
Values may be sent and summed in bfloat16 or wider, within the bound.
A program may use at most 128 MiB of HBM per device.

v0:
```python
import functools

import jax
import jax.numpy as jnp
from jax import lax
from jax.experimental import pallas as pl
from jax.experimental.pallas import tpu as pltpu
from jax.sharding import PartitionSpec as P

GROUPS = 4
SPLIT = 4
MESH = pl.DeviceIdType.MESH


epsilon = 1e-06


def send_back(result):
    return lax.all_to_all(result, "ep", split_axis=0, concat_axis=0, tiled=True)


def general_layer(tokens, norm_gain, route_ids, route_weights, w_gate, w_up, w_down):
    row_count, features = tokens.shape
    top_count = route_ids.shape[1]
    local_experts = w_gate.shape[0]
    ep_size = lax.axis_size("ep")
    experts_all = ep_size * local_experts
    capacity = row_count * GROUPS // experts_all
    floats = tokens.astype(jnp.float32)
    inverse = lax.rsqrt(jnp.mean(floats * floats, axis=1, keepdims=True) + epsilon)
    normed = (floats * inverse * norm_gain).astype(jnp.bfloat16)
    flat_ids = route_ids.reshape(-1)
    onehot = (flat_ids[:, None] == jnp.arange(experts_all, dtype=jnp.int32)[None, :]).astype(
        jnp.int32
    )
    earlier = jnp.cumsum(onehot, axis=0) - onehot
    slot_index = jnp.sum(earlier * onehot, axis=1)
    target = (flat_ids * capacity + slot_index).reshape(row_count, top_count)
    outbound = jnp.zeros((experts_all * capacity, features), jnp.bfloat16)
    for column in range(top_count):
        outbound = outbound.at[target[:, column]].set(normed)
    outbound = outbound.reshape(ep_size, local_experts, capacity, features)
    full_gate, full_up, full_down = (
        lax.all_gather(w_gate, "tp", axis=2, tiled=True),
        lax.all_gather(w_up, "tp", axis=2, tiled=True),
        lax.all_gather(w_down, "tp", axis=1, tiled=True),
    )
    arrived = lax.all_to_all(outbound, "ep", split_axis=0, concat_axis=0, tiled=True)
    gate_pre = jnp.einsum("sjcd,jdf->sjcf", arrived, full_gate, preferred_element_type=jnp.float32)
    up_pre = jnp.einsum("sjcd,jdf->sjcf", arrived, full_up, preferred_element_type=jnp.float32)
    hidden = (jax.nn.silu(gate_pre) * up_pre).astype(jnp.bfloat16)
    result = jnp.einsum("sjcf,jfd->sjcd", hidden, full_down, preferred_element_type=jnp.float32)
    returned_rows = send_back(result.astype(jnp.bfloat16))
    returned_rows = returned_rows.reshape(experts_all * capacity, features)
    combined = jnp.zeros((row_count, features), jnp.float32)
    for column in range(top_count):
        picked = returned_rows[target[:, column]].astype(jnp.float32)
        combined = combined + route_weights[:, column : column + 1] * picked
    return combined.astype(jnp.bfloat16)


def group_kernel(
    members, parts, halves,
    tokens, gain, ids, weights, w_gate, w_up, w_down, out,
    raw, ready, summed, final, place, sent, taken, scales, scales_in, answers, returned,
    gate_all, up_all, down_all, hidden,
    raw_sem, out_sems, own_sems, twin_s, twin_r, peer_s, peer_r, part_s, part_r,
    near_s, near_r, far_s, far_r, row_s, row_r, scale_s, scale_r, back_s, back_r,
):
    part, position, half = lax.axis_index("grp"), lax.axis_index("ep"), lax.axis_index("tp")
    level, member = position // members, position % members
    rows, features = tokens.shape
    slots = sent.shape[1]
    top_count = ids.shape[0]
    peer = {"ep": level * members + (members - 1 - member)}
    other_part = {"grp": parts - 1 - part}
    twin = {"tp": halves - 1 - half}

    def level_of(k):
        return {"ep": (level ^ k) * members + member}

    raw_copy = pltpu.make_async_copy(tokens, raw, raw_sem)
    raw_copy.start()
    barrier = pltpu.get_barrier_semaphore()
    neighbours = [peer, other_part, twin] + [level_of(k) for k in range(1, GROUPS)]
    for device in neighbours:
        pl.semaphore_signal(barrier, inc=1, device_id=device, device_id_type=MESH)

    sources = (w_gate, w_up, w_down)
    stores = (gate_all, up_all, down_all)
    mine = member * halves + half
    theirs = (members - 1 - member) * halves + half

    def remote(src, dst, send, recv, device):
        return pltpu.make_async_remote_copy(
            src_ref=src, dst_ref=dst, send_sem=send, recv_sem=recv,
            device_id=device, device_id_type=MESH,
        )

    pieces = []
    for step in range(SPLIT):
        for tensor in range(3):
            size = sources[tensor].shape[0] // (parts * SPLIT)
            pieces.append((tensor, step, size))

    def span(index, which):
        tensor, step, size = pieces[index]
        start = pl.multiple_of((which * SPLIT + step) * size, size)
        return tensor, pl.ds(start, size)

    def peer_copy(index):
        tensor, window = span(index, part)
        return remote(
            sources[tensor].at[window], stores[tensor].at[mine, window],
            peer_s.at[index], peer_r.at[index], peer,
        )

    def spread_copy(index, which, send, recv, device):
        tensor, window = span(index, which)
        block = stores[tensor].at[theirs, window]
        return remote(block, block, send.at[index], recv.at[index], device)

    peer_copies = [peer_copy(index) for index in range(len(pieces))]
    part_copies = [spread_copy(i, part, part_s, part_r, other_part) for i in range(len(pieces))]
    near_copies = [spread_copy(i, part, near_s, near_r, twin) for i in range(len(pieces))]
    far_copies = [
        spread_copy(i, parts - 1 - part, far_s, far_r, twin) for i in range(len(pieces))
    ]
    own_copies, twin_copies = [], []
    for tensor in range(3):
        own_copies.append(
            pltpu.make_async_copy(sources[tensor], stores[tensor].at[mine], own_sems.at[tensor])
        )
        twin_copies.append(
            remote(
                sources[tensor], stores[tensor].at[mine],
                twin_s.at[tensor], twin_r.at[tensor], twin,
            )
        )
    first = ids[0:1, :]
    group_row = first // members
    lane = lax.broadcasted_iota(jnp.int32, (8, rows), 0)
    mask = (jnp.broadcast_to(group_row, (8, rows)) == lane).astype(jnp.float32)
    before = (
        lax.broadcasted_iota(jnp.int32, (rows, rows), 0)
        < lax.broadcasted_iota(jnp.int32, (rows, rows), 1)
    ).astype(jnp.float32)
    ranks = jnp.dot(
        mask.astype(jnp.bfloat16), before.astype(jnp.bfloat16),
        preferred_element_type=jnp.float32,
    )
    slot_row = jnp.sum(ranks * mask, axis=0, keepdims=True).astype(jnp.int32)
    shares = jnp.zeros((8, rows), jnp.float32)
    for column in range(top_count):
        offset = ids[column : column + 1, :] - group_row * members
        chosen = jnp.broadcast_to(offset, (8, rows)) == lane
        shares = shares + jnp.where(
            chosen, jnp.broadcast_to(weights[column : column + 1, :], (8, rows)), 0.0
        )
    high = shares.astype(jnp.bfloat16)
    rest = shares - high.astype(jnp.float32)
    middle = rest.astype(jnp.bfloat16)
    low = (rest - middle.astype(jnp.float32)).astype(jnp.bfloat16)

    row_copies, scale_copies, back_copies = {}, {}, {}
    slot_iota = lax.broadcasted_iota(jnp.int32, (slots, rows), 0)
    order = (2, 1, 3, 0)
    pl.semaphore_wait(barrier, len(neighbours))
    for copy in peer_copies:
        copy.start()
    raw_copy.wait()
    for k in order:
        key = jnp.where(group_row == (level ^ k), slot_row, -1)
        spots = (jnp.broadcast_to(key, (slots, rows)) == slot_iota).astype(jnp.float32)
        spots = spots.astype(jnp.bfloat16)
        place[k * slots : (k + 1) * slots, :] = spots
        lanes = sum(
            lax.dot_general(
                piece, spots, (((1,), (1,)), ((), ())), preferred_element_type=jnp.float32
            )
            for piece in (high, middle, low)
        )
        packed = taken if k == 0 else sent
        (scales_in if k == 0 else scales)[k] = lanes
        packed[k] = jnp.dot(spots, raw[...], preferred_element_type=jnp.float32).astype(
            jnp.bfloat16
        )
        if k:
            row_copies[k] = remote(sent.at[k], taken.at[k], row_s.at[k], row_r.at[k], level_of(k))
            scale_copies[k] = remote(
                scales.at[k], scales_in.at[k], scale_s.at[k], scale_r.at[k], level_of(k)
            )
            row_copies[k].start()
            scale_copies[k].start()
        if k == order[0]:
            for copy in own_copies + twin_copies:
                copy.start()

    for index in range(len(pieces)):
        peer_copies[index].wait_recv()
        part_copies[index].start()
        near_copies[index].start()
        if index:
            part_copies[index - 1].wait_recv()
            far_copies[index - 1].start()
    part_copies[-1].wait_recv()
    far_copies[-1].start()

    width = gate_all.shape[2]
    diagonal = lax.broadcasted_iota(jnp.int32, (slots, slots), 0) == lax.broadcasted_iota(
        jnp.int32, (slots, slots), 1
    )
    tile = features // GROUPS

    strip = 32

    def norm(k):
        def norm_strip(index, carry):
            window = pl.ds(pl.multiple_of(index * strip, strip), strip)
            floats = taken[k, window, :].astype(jnp.float32)
            inverse = lax.rsqrt(jnp.mean(floats * floats, axis=1, keepdims=True) + epsilon)
            ready[window, :] = (floats * inverse * gain[...]).astype(jnp.bfloat16)
            return carry

        lax.fori_loop(0, slots // strip, norm_strip, 0)

    def widen(k, owner):
        lanes = scales_in[k, pl.ds(owner, 1), :]
        scale = jnp.sum(
            jnp.where(diagonal, jnp.broadcast_to(lanes, (slots, slots)), 0.0),
            axis=1, keepdims=True,
        )
        for side in range(halves):
            block = owner * halves + side
            gate = jnp.dot(ready[...], gate_all[block], preferred_element_type=jnp.float32)
            up = jnp.dot(ready[...], up_all[block], preferred_element_type=jnp.float32)
            hidden[:, pl.ds(pl.multiple_of(block * width, width), width)] = (
                gate / (1.0 + jnp.exp(-gate)) * up * scale
            ).astype(jnp.bfloat16)

    def narrow(k):
        for column in range(features // tile):
            window = slice(column * tile, (column + 1) * tile)
            total = jnp.zeros((slots, tile), jnp.float32)
            for block in range(members * halves):
                total += jnp.dot(
                    hidden[:, block * width : (block + 1) * width],
                    down_all[block, :, window],
                    preferred_element_type=jnp.float32,
                )
            if k:
                answers[k, :, window] = total.astype(jnp.bfloat16)
            else:
                returned[0, :, window] = total.astype(jnp.bfloat16)

    for copy in own_copies:
        copy.wait()
    for copy in twin_copies:
        copy.wait_recv()
    for k in order:
        if k:
            row_copies[k].wait_recv()
            scale_copies[k].wait_recv()
        norm(k)
        widen(k, member)
        if k == order[0]:
            for copy in near_copies + far_copies:
                copy.wait_recv()
        widen(k, members - 1 - member)
        narrow(k)
        if k:
            back_copies[k] = remote(
                answers.at[k], returned.at[k], back_s.at[k], back_r.at[k], level_of(k)
            )
            back_copies[k].start()

    def unpack(k, window):
        return lax.dot_general(
            place[k * slots : (k + 1) * slots, :], returned[k, :, window],
            (((0,), (0,)), ((), ())), preferred_element_type=jnp.float32,
        )

    tiles = [slice(start, start + tile) for start in range(0, features, tile)]
    for window in tiles:
        summed[:, window] = unpack(0, window)
    out_copies = []
    for k in order[:-1]:
        back_copies[k].wait_recv()
        for window in tiles:
            total = summed[:, window] + unpack(k, window)
            if k == order[-2]:
                final[:, window] = total.astype(jnp.bfloat16)
                copy = pltpu.make_async_copy(
                    final.at[:, window], out.at[:, window], out_sems.at[window.start // tile]
                )
                copy.start()
                out_copies.append(copy)
            else:
                summed[:, window] = total

    for copy in peer_copies + part_copies + near_copies + far_copies + twin_copies:
        copy.wait_send()
    for k in (1, 2, 3):
        row_copies[k].wait_send()
        scale_copies[k].wait_send()
        back_copies[k].wait_send()
    for copy in out_copies:
        copy.wait()


def group_layer(members, tokens, norm_gain, route_ids, route_weights, w_gate, w_up, w_down):
    rows, features = tokens.shape
    parts, halves = lax.axis_size("grp"), lax.axis_size("tp")
    width = w_gate.shape[2]
    slots = rows // route_ids.shape[1]
    copies = 3 * SPLIT
    blocks = members * halves
    bf16, f32, dma = jnp.bfloat16, jnp.float32, pltpu.SemaphoreType.DMA
    vmem, anywhere = pl.BlockSpec(memory_space=pltpu.VMEM), pl.BlockSpec(memory_space=pl.ANY)
    return pl.pallas_call(
        functools.partial(group_kernel, members, parts, halves),
        out_shape=jax.ShapeDtypeStruct((rows, features), bf16),
        in_specs=[anywhere] + [vmem] * 3 + [anywhere] * 3,
        out_specs=anywhere,
        scratch_shapes=[
            pltpu.VMEM((rows, features), bf16),
            pltpu.VMEM((slots, features), bf16),
            pltpu.VMEM((rows, features), f32),
            pltpu.VMEM((rows, features), bf16),
            pltpu.VMEM((GROUPS * slots, rows), bf16),
            pltpu.VMEM((GROUPS, slots, features), bf16),
            pltpu.VMEM((GROUPS, slots, features), bf16),
            pltpu.VMEM((GROUPS, 8, slots), f32),
            pltpu.VMEM((GROUPS, 8, slots), f32),
            pltpu.VMEM((GROUPS, slots, features), bf16),
            pltpu.VMEM((GROUPS, slots, features), bf16),
            pltpu.VMEM((blocks, features, width), bf16),
            pltpu.VMEM((blocks, features, width), bf16),
            pltpu.VMEM((blocks, width, features), bf16),
            pltpu.VMEM((slots, blocks * width), bf16),
            dma, dma((GROUPS,)), dma((3,)), dma((3,)), dma((3,)),
        ]
        + [dma((copies,)) for _ in range(8)]
        + [dma((GROUPS,)) for _ in range(6)],
        compiler_params=pltpu.CompilerParams(
            collective_id=0, has_side_effects=True, vmem_limit_bytes=63 * 1024 * 1024
        ),
    )(
        tokens, norm_gain.reshape(1, features), route_ids.T, route_weights.T,
        w_gate[0], w_up[0], w_down[0],
    )


def solution(mesh):
    sizes = mesh.shape

    def per_device(tokens, norm_gain, route_ids, route_weights, w_gate, w_up, w_down):
        arguments = (tokens, norm_gain, route_ids, route_weights, w_gate, w_up, w_down)
        members = sizes["ep"] * w_gate.shape[0] // GROUPS
        paired = members == route_ids.shape[1] == sizes["grp"] == sizes["tp"] == 2
        if paired and w_gate.shape[0] == 1:
            return group_layer(members, *arguments)
        return general_layer(*arguments)

    in_specs = (
        P(("grp", "ep", "tp"), None),
        P(),
        P(("grp", "ep", "tp"), None),
        P(("grp", "ep", "tp"), None),
        P("ep", None, "tp"),
        P("ep", None, "tp"),
        P("ep", "tp", None),
    )
    out_specs = P(("grp", "ep", "tp"), None)
    return jax.shard_map(
        per_device, mesh=mesh, in_specs=in_specs, out_specs=out_specs, check_vma=False
    )
```

profile of v0, /device:TPU:8, one launch (start us, length us, event | category | flops | bytes accessed | tf_op | source)
XLA Modules:
  0.0 99.7 jit_solution(6331734582495967221)
XLA Ops:
  0.0 97.4 %shard_map.73 = bf16[256,2048]{1,0:T(8,128)(2,1)} custom-call(bf16[256,2048]{1,0:T(8,128)(2,1)} %tokens.1, f32[1,2048]{1,0:T(1,128)} %bitcast.9, s32[2,256]{1,0:T(2,128)} %bitcast.10, f32[2,256]{1,0:T(2,128)} %bitcast.11, bf16[2048,256]{1,0:T(8,128)(2,1)} %bitcast.6, bf16[2048,256]{1,0:T(8,128)(2,1)} %bitcast.7, bf16[256,2048]{1,0:T(8,128)(2,1)} %bitcast.8), custom_call_target="tpu_custom_call" | custom-call | tf_op jit(solution)/shard_map/pallas_call | solution.py:320
  97.4 2.3 %copy.9 = bf16[256,2048]{1,0:T(8,128)(2,1)} copy(bf16[256,2048]{1,0:T(8,128)(2,1)} %shard_map.73) | data formatting | bytes 2097152
where the time goes:
time: 99.9 us; the launch traced here: 99.7 us
  Pallas kernels  97.4 us (97%)
  local copies, waits for them, and re-layouts  2.3 us (2%)
    pallas_call x1, Pallas kernels, group_layer(): pl.pallas_call(functools.partial(group_kernel, members, parts, halves), o...  97.4 us
    unnamed x1, local copies, waits for them, and re-layouts  2.3 us

commit v1 on v0

--- a/solution.py
+++ b/solution.py
@@ -8,6 +8,7 @@
 from jax.sharding import PartitionSpec as P
 
 GROUPS = 4
+EARLY = 1
 SPLIT = 4
 MESH = pl.DeviceIdType.MESH
 
@@ -61,10 +62,10 @@
 
 def group_kernel(
     members, parts, halves,
-    tokens, gain, ids, weights, w_gate, w_up, w_down, out,
-    raw, ready, summed, final, place, sent, taken, scales, scales_in, answers, returned,
+    tokens, gain_in, ids_in, weights_in, w_gate, w_up, w_down, out,
+    gain, ids, weights, raw, ready, summed, place, sent, taken, scales, scales_in, answers, returned,
     gate_all, up_all, down_all, hidden,
-    raw_sem, out_sems, own_sems, twin_s, twin_r, peer_s, peer_r, part_s, part_r,
+    raw_sem, small_sems, own_sems, twin_s, twin_r, peer_s, peer_r, part_s, part_r,
     near_s, near_r, far_s, far_r, row_s, row_r, scale_s, scale_r, back_s, back_r,
 ):
     part, position, half = lax.axis_index("grp"), lax.axis_index("ep"), lax.axis_index("tp")
@@ -79,12 +80,17 @@
     def level_of(k):
         return {"ep": (level ^ k) * members + member}
 
-    raw_copy = pltpu.make_async_copy(tokens, raw, raw_sem)
-    raw_copy.start()
     barrier = pltpu.get_barrier_semaphore()
-    neighbours = [peer, other_part, twin] + [level_of(k) for k in range(1, GROUPS)]
+    neighbours = [level_of(k) for k in range(GROUPS - 1, 0, -1)] + [peer, other_part, twin]
     for device in neighbours:
         pl.semaphore_signal(barrier, inc=1, device_id=device, device_id_type=MESH)
+    small_copies = [
+        pltpu.make_async_copy(src, dst, small_sems.at[i])
+        for i, (src, dst) in enumerate(((ids_in, ids), (weights_in, weights), (gain_in, gain)))
+    ]
+    raw_copy = pltpu.make_async_copy(tokens, raw, raw_sem)
+    for copy in small_copies + [raw_copy]:
+        copy.start()
 
     sources = (w_gate, w_up, w_down)
     stores = (gate_all, up_all, down_all)
@@ -137,6 +143,8 @@
                 twin_s.at[tensor], twin_r.at[tensor], twin,
             )
         )
+    for copy in small_copies:
+        copy.wait()
     first = ids[0:1, :]
     group_row = first // members
     lane = lax.broadcasted_iota(jnp.int32, (8, rows), 0)
@@ -165,11 +173,13 @@
     row_copies, scale_copies, back_copies = {}, {}, {}
     slot_iota = lax.broadcasted_iota(jnp.int32, (slots, rows), 0)
     order = (2, 1, 3, 0)
-    pl.semaphore_wait(barrier, len(neighbours))
-    for copy in peer_copies:
-        copy.start()
-    raw_copy.wait()
-    for k in order:
+    for k in (1, 2, 3):
+        row_copies[k] = remote(sent.at[k], taken.at[k], row_s.at[k], row_r.at[k], level_of(k))
+        scale_copies[k] = remote(
+            scales.at[k], scales_in.at[k], scale_s.at[k], scale_r.at[k], level_of(k)
+        )
+
+    def pack(k):
         key = jnp.where(group_row == (level ^ k), slot_row, -1)
         spots = (jnp.broadcast_to(key, (slots, rows)) == slot_iota).astype(jnp.float32)
         spots = spots.astype(jnp.bfloat16)
@@ -185,15 +195,19 @@
         packed[k] = jnp.dot(spots, raw[...], preferred_element_type=jnp.float32).astype(
             jnp.bfloat16
         )
+
+    raw_copy.wait()
+    for k in order[:EARLY]:
+        pack(k)
+    pl.semaphore_wait(barrier, len(neighbours))
+    for k in order:
+        if k not in order[:EARLY]:
+            pack(k)
         if k:
-            row_copies[k] = remote(sent.at[k], taken.at[k], row_s.at[k], row_r.at[k], level_of(k))
-            scale_copies[k] = remote(
-                scales.at[k], scales_in.at[k], scale_s.at[k], scale_r.at[k], level_of(k)
-            )
             row_copies[k].start()
             scale_copies[k].start()
         if k == order[0]:
-            for copy in own_copies + twin_copies:
+            for copy in peer_copies + own_copies + twin_copies:
                 copy.start()
 
     for index in range(len(pieces)):
@@ -283,18 +297,12 @@
     tiles = [slice(start, start + tile) for start in range(0, features, tile)]
     for window in tiles:
         summed[:, window] = unpack(0, window)
-    out_copies = []
     for k in order[:-1]:
         back_copies[k].wait_recv()
         for window in tiles:
             total = summed[:, window] + unpack(k, window)
             if k == order[-2]:
-                final[:, window] = total.astype(jnp.bfloat16)
-                copy = pltpu.make_async_copy(
-                    final.at[:, window], out.at[:, window], out_sems.at[window.start // tile]
-                )
-                copy.start()
-                out_copies.append(copy)
+                out[:, window] = total.astype(jnp.bfloat16)
             else:
                 summed[:, window] = total
 
@@ -304,8 +312,6 @@
         row_copies[k].wait_send()
         scale_copies[k].wait_send()
         back_copies[k].wait_send()
-    for copy in out_copies:
-        copy.wait()
 
 
 def group_layer(members, tokens, norm_gain, route_ids, route_weights, w_gate, w_up, w_down):
@@ -316,17 +322,19 @@
     copies = 3 * SPLIT
     blocks = members * halves
     bf16, f32, dma = jnp.bfloat16, jnp.float32, pltpu.SemaphoreType.DMA
-    vmem, anywhere = pl.BlockSpec(memory_space=pltpu.VMEM), pl.BlockSpec(memory_space=pl.ANY)
+    vmem = pl.BlockSpec(memory_space=pltpu.VMEM)
     return pl.pallas_call(
         functools.partial(group_kernel, members, parts, halves),
-        out_shape=jax.ShapeDtypeStruct((rows, features), bf16),
-        in_specs=[anywhere] + [vmem] * 3 + [anywhere] * 3,
-        out_specs=anywhere,
+        out_shape=pltpu.VMEM((rows, features), bf16),
+        in_specs=[pl.BlockSpec(memory_space=pltpu.HBM)] * 7,
+        out_specs=vmem,
         scratch_shapes=[
+            pltpu.VMEM((1, features), f32),
+            pltpu.VMEM(route_ids.shape[::-1], jnp.int32),
+            pltpu.VMEM(route_ids.shape[::-1], f32),
             pltpu.VMEM((rows, features), bf16),
             pltpu.VMEM((slots, features), bf16),
             pltpu.VMEM((rows, features), f32),
-            pltpu.VMEM((rows, features), bf16),
             pltpu.VMEM((GROUPS * slots, rows), bf16),
             pltpu.VMEM((GROUPS, slots, features), bf16),
             pltpu.VMEM((GROUPS, slots, features), bf16),
@@ -338,12 +346,12 @@
             pltpu.VMEM((blocks, features, width), bf16),
             pltpu.VMEM((blocks, width, features), bf16),
             pltpu.VMEM((slots, blocks * width), bf16),
-            dma, dma((GROUPS,)), dma((3,)), dma((3,)), dma((3,)),
+            dma, dma((3,)), dma((3,)), dma((3,)), dma((3,)),
         ]
         + [dma((copies,)) for _ in range(8)]
         + [dma((GROUPS,)) for _ in range(6)],
         compiler_params=pltpu.CompilerParams(
-            collective_id=0, has_side_effects=True, vmem_limit_bytes=63 * 1024 * 1024
+            collective_id=0, has_side_effects=True, vmem_limit_bytes=64400 * 1024
         ),
     )(
         tokens, norm_gain.reshape(1, features), route_ids.T, route_weights.T,

time: 99.9 us -> 97.1 us (0.972)
  Pallas kernels: 97.4 us -> 95.9 us
  local copies, waits for them, and re-layouts: 2.3 us -> 0.97 us
    pallas_call x1, Pallas kernels: 97.4 us -> 95.9 us  [group_layer(): pl.pallas_call(functools.partial(group_kernel, members, parts, halves), o...]
    unnamed x1, local copies, waits for them, and re-layouts: 2.3 us -> 0.97 us
where the time goes in v1:
time: 97.1 us; the launch traced here: 96.9 us
  Pallas kernels  95.9 us (99%)
    pallas_call x1, Pallas kernels, group_layer(): pl.pallas_call(functools.partial(group_kernel, members, parts, halves), o...  95.9 us

profile of v1, /device:TPU:8, one launch (start us, length us, event | category | flops | bytes accessed | tf_op | source)
XLA Modules:
  0.0 96.9 jit_solution(14128612915437716124)
XLA Ops:
  0.0 95.9 %shard_map.73 = bf16[256,2048]{1,0:T(8,128)(2,1)S(1)} custom-call(bf16[256,2048]{1,0:T(8,128)(2,1)} %tokens.1, f32[1,2048]{1,0:T(1,128)} %bitcast.9, s32[2,256]{1,0:T(2,128)} %bitcast.10, f32[2,256]{1,0:T(2,128)} %bitcast.11, bf16[2048,256]{1,0:T(8,128)(2,1)} %bitcast.6, bf16[2048,256]{1,0:T(8,128)(2,1)} %bitcast.7, bf16[256,2048]{1,0:T(8,128)(2,1)} %bitcast.8), custom_call_target="tpu_custom_call" | custom-call | tf_op jit(solution)/shard_map/pallas_call | solution.py:326
  95.9 1.0 %copy.9 = bf16[256,2048]{1,0:T(8,128)(2,1)} copy(bf16[256,2048]{1,0:T(8,128)(2,1)S(1)} %shard_map.73) | data formatting | bytes 2097152

commit v2 on v1

v2 whole, which is shorter than its diff:
```python
import functools

import jax
import jax.numpy as jnp
from jax import lax
from jax.experimental import pallas as pl
from jax.experimental.pallas import tpu as pltpu
from jax.sharding import PartitionSpec as P

GROUPS = 4
SPLIT = 4
SWAP_AT = 11
MESH = pl.DeviceIdType.MESH


epsilon = 1e-06


def send_back(result):
    return lax.all_to_all(result, "ep", split_axis=0, concat_axis=0, tiled=True)


def general_layer(tokens, norm_gain, route_ids, route_weights, w_gate, w_up, w_down):
    row_count, features = tokens.shape
    top_count = route_ids.shape[1]
    local_experts = w_gate.shape[0]
    ep_size = lax.axis_size("ep")
    experts_all = ep_size * local_experts
    capacity = row_count * GROUPS // experts_all
    floats = tokens.astype(jnp.float32)
    inverse = lax.rsqrt(jnp.mean(floats * floats, axis=1, keepdims=True) + epsilon)
    normed = (floats * inverse * norm_gain).astype(jnp.bfloat16)
    flat_ids = route_ids.reshape(-1)
    onehot = (flat_ids[:, None] == jnp.arange(experts_all, dtype=jnp.int32)[None, :]).astype(
        jnp.int32
    )
    earlier = jnp.cumsum(onehot, axis=0) - onehot
    slot_index = jnp.sum(earlier * onehot, axis=1)
    target = (flat_ids * capacity + slot_index).reshape(row_count, top_count)
    outbound = jnp.zeros((experts_all * capacity, features), jnp.bfloat16)
    for column in range(top_count):
        outbound = outbound.at[target[:, column]].set(normed)
    outbound = outbound.reshape(ep_size, local_experts, capacity, features)
    full_gate, full_up, full_down = (
        lax.all_gather(w_gate, "tp", axis=2, tiled=True),
        lax.all_gather(w_up, "tp", axis=2, tiled=True),
        lax.all_gather(w_down, "tp", axis=1, tiled=True),
    )
    arrived = lax.all_to_all(outbound, "ep", split_axis=0, concat_axis=0, tiled=True)
    gate_pre = jnp.einsum("sjcd,jdf->sjcf", arrived, full_gate, preferred_element_type=jnp.float32)
    up_pre = jnp.einsum("sjcd,jdf->sjcf", arrived, full_up, preferred_element_type=jnp.float32)
    hidden = (jax.nn.silu(gate_pre) * up_pre).astype(jnp.bfloat16)
    result = jnp.einsum("sjcf,jfd->sjcd", hidden, full_down, preferred_element_type=jnp.float32)
    returned_rows = send_back(result.astype(jnp.bfloat16))
    returned_rows = returned_rows.reshape(experts_all * capacity, features)
    combined = jnp.zeros((row_count, features), jnp.float32)
    for column in range(top_count):
        picked = returned_rows[target[:, column]].astype(jnp.float32)
        combined = combined + route_weights[:, column : column + 1] * picked
    return combined.astype(jnp.bfloat16)


def group_kernel(
    members, parts, halves,
    tokens, gain_in, ids_in, weights_in, w_gate, w_up, w_down, out,
    gain, ids, weights, raw, ready, summed, place, sent, taken, scales, scales_in, answers,
    returned, gate_all, up_all, down_all, hidden,
    own_gate, own_up, own_down, peer_rows, peer_scales, partial, parts_out, parts_in,
    raw_sem, small_sems, own_sems, twin_s, twin_r, peer_s, peer_r, part_s, part_r,
    near_s, near_r, far_s, far_r, guest_s, guest_r, cross_s, cross_r,
    gnear_s, gnear_r, gfar_s, gfar_r, row_s, row_r, scale_s, scale_r, back_s, back_r,
    swap_s, swap_r, note_s, note_r, half_s, half_r,
):
    part, position, half = lax.axis_index("grp"), lax.axis_index("ep"), lax.axis_index("tp")
    level, member = position // members, position % members
    inner = ((level + 1) // 2) % 2
    rows, features = tokens.shape
    slots = sent.shape[1]
    top_count = ids.shape[0]
    peer = {"ep": level * members + (members - 1 - member)}
    other_part = {"grp": parts - 1 - part}
    twin = {"tp": halves - 1 - half}

    def level_of(k):
        return {"ep": (level ^ k) * members + member}

    on_inner, on_outer = pl.when(inner == 1), pl.when(inner == 0)

    barrier = pltpu.get_barrier_semaphore()
    neighbours = [level_of(k) for k in range(GROUPS - 1, 0, -1)] + [peer, other_part, twin]
    for device in neighbours:
        pl.semaphore_signal(barrier, inc=1, device_id=device, device_id_type=MESH)
    small_copies = [
        pltpu.make_async_copy(src, dst, small_sems.at[i])
        for i, (src, dst) in enumerate(((ids_in, ids), (weights_in, weights), (gain_in, gain)))
    ]
    raw_copy = pltpu.make_async_copy(tokens, raw, raw_sem)
    for copy in small_copies + [raw_copy]:
        copy.start()

    sources = (w_gate, w_up, w_down)
    stores = (gate_all, up_all, down_all)
    own_stores = (own_gate, own_up, own_down)
    mine = member * halves + half
    theirs = (members - 1 - member) * halves + half

    def remote(src, dst, send, recv, device):
        return pltpu.make_async_remote_copy(
            src_ref=src, dst_ref=dst, send_sem=send, recv_sem=recv,
            device_id=device, device_id_type=MESH,
        )

    pieces = [(tensor, step) for step in range(SPLIT) for tensor in range(2)]
    pieces += [(2, step) for step in range(SPLIT)]
    count = len(pieces)
    wide = 2 * SPLIT

    def window_of(piece, which):
        tensor, step = piece
        size = sources[tensor].shape[0] // (parts * SPLIT)
        return pl.ds(pl.multiple_of((which * SPLIT + step) * size, size), size)

    def first_copies(send, recv, device):
        copies = []
        for i, piece in enumerate(pieces):
            window = window_of(piece, part)
            copies.append(remote(
                sources[piece[0]].at[window], stores[piece[0]].at[mine, window],
                send.at[i], recv.at[i], device,
            ))
        return copies

    def spread_copies(block, which, send, recv, device):
        copies = []
        for i, piece in enumerate(pieces):
            held = stores[piece[0]].at[block, window_of(piece, which)]
            copies.append(remote(held, held, send.at[i], recv.at[i], device))
        return copies

    other = parts - 1 - part
    peer_copies = first_copies(peer_s, peer_r, peer)
    relay_copies = spread_copies(mine, part, peer_s, peer_r, peer)
    part_copies = spread_copies(theirs, part, part_s, part_r, other_part)
    near_copies = spread_copies(theirs, part, near_s, near_r, twin)
    far_copies = spread_copies(theirs, other, far_s, far_r, twin)
    guest_copies = first_copies(guest_s, guest_r, level_of(GROUPS - 1))
    cross_copies = spread_copies(mine, part, cross_s, cross_r, other_part)
    gnear_copies = spread_copies(mine, part, gnear_s, gnear_r, twin)
    gfar_copies = spread_copies(mine, other, gfar_s, gfar_r, twin)

    def home_copies(targets, block):
        copies, twins = [], []
        for tensor in range(3):
            target = targets[tensor].at[block]
            copies.append(
                pltpu.make_async_copy(sources[tensor], target, own_sems.at[tensor])
            )
            twins.append(
                remote(sources[tensor], target, twin_s.at[tensor], twin_r.at[tensor], twin)
            )
        return copies, twins

    group_copies, group_twins = home_copies(stores, mine)
    own_copies, own_twins = home_copies(own_stores, half)
    row_to = {1: level_of(1), 2: level_of(1 + inner), 3: level_of(3)}
    back_to = {1: level_of(1), 2: level_of(2 - inner), 3: level_of(3)}
    tile = features // GROUPS
    tiles = [slice(begin, begin + tile) for begin in range(0, features, tile)]

    def tiled_copies(src, dst, send, recv, base, device):
        return [
            remote(
                src.at[:, window], dst.at[:, window],
                send.at[base * GROUPS + t], recv.at[base * GROUPS + t], device,
            )
            for t, window in enumerate(tiles)
        ]

    row_copies, scale_copies, back_copies = {}, {}, {}
    for k in (1, 2, 3):
        row_copies[k] = tiled_copies(sent.at[k], taken.at[k], row_s, row_r, k, row_to[k])
        scale_copies[k] = remote(
            scales.at[k], scales_in.at[k], scale_s.at[k], scale_r.at[k], row_to[k]
        )
        back_copies[k] = tiled_copies(answers.at[k], returned.at[k], back_s, back_r, k, back_to[k])
    swap_copies, note_copies, half_copies = [], [], []
    for j, k in enumerate((1, 0)):
        swap_copies.append(tiled_copies(taken.at[k], peer_rows.at[j], swap_s, swap_r, j, peer))
        note_copies.append(
            remote(scales_in.at[k], peer_scales.at[j], note_s.at[j], note_r.at[j], peer)
        )
        half_copies.append(tiled_copies(parts_out.at[j], parts_in.at[j], half_s, half_r, j, peer))

    for copy in small_copies:
        copy.wait()
    first = ids[0:1, :]
    group_row = first // members
    lane = lax.broadcasted_iota(jnp.int32, (8, rows), 0)
    mask = (jnp.broadcast_to(group_row, (8, rows)) == lane).astype(jnp.float32)
    before = (
        lax.broadcasted_iota(jnp.int32, (rows, rows), 0)
        < lax.broadcasted_iota(jnp.int32, (rows, rows), 1)
    ).astype(jnp.float32)
    ranks = jnp.dot(
        mask.astype(jnp.bfloat16), before.astype(jnp.bfloat16),
        preferred_element_type=jnp.float32,
    )
    slot_row = jnp.sum(ranks * mask, axis=0, keepdims=True).astype(jnp.int32)
    shares = jnp.zeros((8, rows), jnp.float32)
    for column in range(top_count):
        offset = ids[column : column + 1, :] - group_row * members
        chosen = jnp.broadcast_to(offset, (8, rows)) == lane
        shares = shares + jnp.where(
            chosen, jnp.broadcast_to(weights[column : column + 1, :], (8, rows)), 0.0
        )
    high = shares.astype(jnp.bfloat16)
    rest = shares - high.astype(jnp.float32)
    middle = rest.astype(jnp.bfloat16)
    low = (rest - middle.astype(jnp.float32)).astype(jnp.bfloat16)
    slot_iota = lax.broadcasted_iota(jnp.int32, (slots, rows), 0)

    def pack(k):
        key = jnp.where(group_row == (level ^ k), slot_row, -1)
        spots = (jnp.broadcast_to(key, (slots, rows)) == slot_iota).astype(jnp.float32)
        spots = spots.astype(jnp.bfloat16)
        place[k * slots : (k + 1) * slots, :] = spots
        lanes = sum(
            lax.dot_general(
                piece, spots, (((1,), (1,)), ((), ())), preferred_element_type=jnp.float32
            )
            for piece in (high, middle, low)
        )
        packed = taken if k == 0 else sent
        (scales_in if k == 0 else scales)[k] = lanes
        packed[k] = jnp.dot(spots, raw[...], preferred_element_type=jnp.float32).astype(
            jnp.bfloat16
        )

    def start(copies):
        for copy in copies:
            copy.start()

    def land(copies):
        for copy in copies:
            copy.wait_recv()

    def leave(copies):
        for copy in copies:
            copy.wait_send()

    def send(k):
        scale_copies[k].start()
        start(row_copies[k])

    def arrive(k):
        land(row_copies[k] + [scale_copies[k]])

    raw_copy.wait()
    pack(1)
    pl.semaphore_wait(barrier, len(neighbours))

    @on_inner
    def _():
        start(guest_copies)

    send(1)

    @on_outer
    def _():
        start(peer_copies)

    pack(0)

    @on_inner
    def _():
        start(own_copies + own_twins)

    @on_outer
    def _():
        start(group_copies + group_twins)

    pack(2)
    send(2)
    pack(3)

    width = gate_all.shape[2]
    diagonal = lax.broadcasted_iota(jnp.int32, (slots, slots), 0) == lax.broadcasted_iota(
        jnp.int32, (slots, slots), 1
    )
    strip = 32

    def norm(source, base):
        def norm_strip(index, carry):
            start = pl.multiple_of(index * strip, strip)
            floats = source[pl.ds(start, strip), :].astype(jnp.float32)
            inverse = lax.rsqrt(jnp.mean(floats * floats, axis=1, keepdims=True) + epsilon)
            ready[pl.ds(base + start, strip), :] = (floats * inverse * gain[...]).astype(
                jnp.bfloat16
            )
            return carry

        lax.fori_loop(0, slots // strip, norm_strip, 0)

    def column_of(share, owner):
        return jnp.sum(
            jnp.where(diagonal, jnp.broadcast_to(share[pl.ds(owner, 1), :], (slots, slots)), 0.0),
            axis=1, keepdims=True,
        )

    def widen(base, shares_in, owner, gate_block, up_block, column):
        scale = jnp.concatenate([column_of(share, owner) for share in shares_in], axis=0)
        size = slots * len(shares_in)
        values = ready[base : base + size, :]
        gate = jnp.dot(values, gate_block[...], preferred_element_type=jnp.float32)
        up = jnp.dot(values, up_block[...], preferred_element_type=jnp.float32)
        hidden[base : base + size, pl.ds(pl.multiple_of(column * width, width), width)] = (
            gate / (1.0 + jnp.exp(-gate)) * up * scale
        ).astype(jnp.bfloat16)

    def widen_group(base, shares_in, owner, side):
        block = owner * halves + side
        widen(base, shares_in, owner, gate_all.at[block], up_all.at[block], block)

    def narrow(base, size, blocks, column):
        window = slice(column * tile, (column + 1) * tile)
        total = jnp.zeros((size, tile), jnp.float32)
        for index, block in enumerate(blocks):
            total += jnp.dot(
                hidden[base : base + size, index * width : (index + 1) * width],
                block[:, window], preferred_element_type=jnp.float32,
            )
        return window, total

    group_down = [down_all.at[block] for block in range(members * halves)]

    def narrow_group(base, targets):
        for column in range(len(tiles)):
            window, total = narrow(base, slots * len(targets), group_down, column)
            for j, (target, copies) in enumerate(targets):
                target[:, window] = total[j * slots : (j + 1) * slots].astype(jnp.bfloat16)
                if copies:
                    copies[column].start()

    def whole(pair, base):
        for j, k in enumerate(pair):
            norm(taken.at[k], base + j * slots)
        for owner in range(members):
            for side in range(halves):
                widen_group(base, [scales_in.at[k] for k in pair], owner, side)
        narrow_group(
            base, [((answers if k else returned).at[k], back_copies.get(k)) for k in pair]
        )

    def divided(j, k):
        base = 2 * slots * j
        norm(peer_rows.at[j], base)
        norm(taken.at[k], base + slots)
        for side in range(halves):
            widen(
                base, [peer_scales.at[j], scales_in.at[k]], member,
                own_gate.at[side], own_up.at[side], side,
            )
        blocks = [own_down.at[side] for side in range(halves)]
        for column in range(len(tiles)):
            window, total = narrow(base, 2 * slots, blocks, column)
            parts_out[j, :, window] = total[:slots].astype(jnp.bfloat16)
            half_copies[j][column].start()
            partial[j, :, window] = total[slots:]

    def joined(j, column, target, copies=None):
        half_copies[j][column].wait_recv()
        window = tiles[column]
        target[:, window] = (
            partial[j, :, window] + parts_in[j, :, window].astype(jnp.float32)
        ).astype(jnp.bfloat16)
        if copies:
            copies[column].start()

    def unpack(k, window):
        return lax.dot_general(
            place[k * slots : (k + 1) * slots, :], returned[k, :, window],
            (((0,), (0,)), ((), ())), preferred_element_type=jnp.float32,
        )

    def add(k, fresh=False):
        for window in tiles:
            value = unpack(k, window)
            summed[:, window] = value if fresh else summed[:, window] + value

    def back(k):
        for t, window in enumerate(tiles):
            back_copies[k][t].wait_recv()
            summed[:, window] = summed[:, window] + unpack(k, window)

    def finish(k):
        for t, window in enumerate(tiles):
            back_copies[k][t].wait_recv()
            out[:, window] = (summed[:, window] + unpack(k, window)).astype(jnp.bfloat16)

    @on_outer
    def _():
        for i in range(count):
            peer_copies[i].wait_recv()
            part_copies[i].start()
            near_copies[i].start()
            if i:
                part_copies[i - 1].wait_recv()
                far_copies[i - 1].start()
        part_copies[-1].wait_recv()
        far_copies[-1].start()
        for copy in group_copies:
            copy.wait()
        land(group_twins + near_copies + far_copies)
        arrive(1)
        whole((1, 0), 2 * slots)
        send(3)
        add(0, True)
        arrive(2)
        whole((2,), 0)
        arrive(3)
        whole((3,), slots)
        back(1)
        back(3)
        finish(2)
        leave(peer_copies + group_twins + row_copies[3] + [scale_copies[3]] + back_copies[3])

    @on_inner
    def _():
        def take(i):
            guest_copies[i].wait_recv()
            cross_copies[i].start()
            gnear_copies[i].start()

        scale_copies[1].wait_recv()
        note_copies[0].start()
        for i in range(GROUPS):
            row_copies[1][i].wait_recv()
            swap_copies[0][i].start()
            take(i)
        relay_copies[0].start()
        take(GROUPS)
        for copy in own_copies:
            copy.wait()
        land(own_twins + swap_copies[0] + note_copies[:1])
        divided(0, 1)
        start(relay_copies[1 : GROUPS + 1])
        for i in range(GROUPS + 1, count):
            take(i)
            relay_copies[i].start()
            column = i - GROUPS - 1
            if column < GROUPS:
                joined(0, column, answers.at[1], back_copies[1])
            if i == SWAP_AT:
                note_copies[1].start()
                start(swap_copies[1])
        arrive(2)
        shares_in = [scales_in.at[2], scales.at[3]]
        norm(taken.at[2], 0)
        norm(sent.at[3], slots)
        for i in range(count):
            peer_copies[i].wait_recv()
            part_copies[i].start()
            near_copies[i].start()
            cross_copies[i].wait_recv()
            gfar_copies[i].start()
            if i:
                part_copies[i - 1].wait_recv()
                far_copies[i - 1].start()
            if i == wide:
                land(gnear_copies[:wide] + gfar_copies[:wide])
            if i == wide + members:
                land(near_copies[:wide] + far_copies[:wide])
            if i >= wide:
                owner, side = (i - wide) // halves, (i - wide) % halves
                widen_group(0, shares_in, (member + owner) % members, side)
        part_copies[-1].wait_recv()
        far_copies[-1].start()
        land(
            gnear_copies[wide:] + gfar_copies[wide:] + near_copies[wide:] + far_copies[wide:]
        )
        narrow_group(0, [(answers.at[2], back_copies[2]), (returned.at[3], None)])
        land(swap_copies[1] + note_copies[1:])
        divided(1, 0)
        add(3, True)
        back(1)
        back(2)
        for column, window in enumerate(tiles):
            joined(1, column, returned.at[0])
            out[:, window] = (summed[:, window] + unpack(0, window)).astype(jnp.bfloat16)
        leave(guest_copies + cross_copies + gnear_copies + gfar_copies + relay_copies)
        leave(own_twins + note_copies)
        for j in range(2):
            leave(swap_copies[j] + half_copies[j])

    leave(part_copies + near_copies + far_copies)
    for k in (1, 2):
        leave(row_copies[k] + [scale_copies[k]] + back_copies[k])


def group_layer(members, tokens, norm_gain, route_ids, route_weights, w_gate, w_up, w_down):
    rows, features = tokens.shape
    parts, halves = lax.axis_size("grp"), lax.axis_size("tp")
    width = w_gate.shape[2]
    slots = rows // route_ids.shape[1]
    copies = 3 * SPLIT
    blocks = members * halves
    bf16, f32, dma = jnp.bfloat16, jnp.float32, pltpu.SemaphoreType.DMA

    def vmem(*shape, dtype=bf16):
        return pltpu.VMEM(shape, dtype)

    return pl.pallas_call(
        functools.partial(group_kernel, members, parts, halves),
        out_shape=vmem(rows, features),
        in_specs=[pl.BlockSpec(memory_space=pltpu.HBM)] * 7,
        out_specs=pl.BlockSpec(memory_space=pltpu.VMEM),
        scratch_shapes=[
            vmem(1, features, dtype=f32),
            vmem(*route_ids.shape[::-1], dtype=jnp.int32),
            vmem(*route_ids.shape[::-1], dtype=f32),
            vmem(rows, features),
            vmem(GROUPS * slots, features),
            vmem(rows, features, dtype=f32),
            vmem(GROUPS * slots, rows),
            vmem(GROUPS, slots, features),
            vmem(GROUPS, slots, features),
            vmem(GROUPS, 8, slots, dtype=f32),
            vmem(GROUPS, 8, slots, dtype=f32),
            vmem(GROUPS, slots, features),
            vmem(GROUPS, slots, features),
            vmem(blocks, features, width),
            vmem(blocks, features, width),
            vmem(blocks, width, features),
            vmem(GROUPS * slots, blocks * width),
            vmem(halves, features, width),
            vmem(halves, features, width),
            vmem(halves, width, features),
            vmem(2, slots, features),
            vmem(2, 8, slots, dtype=f32),
            vmem(2, slots, features, dtype=f32),
            vmem(2, slots, features),
            vmem(2, slots, features),
            dma, dma((3,)), dma((3,)), dma((3,)), dma((3,)),
        ]
        + [dma((copies,)) for _ in range(16)]
        + [dma((GROUPS * GROUPS,)) for _ in range(2)]
        + [dma((GROUPS,)) for _ in range(2)]
        + [dma((GROUPS * GROUPS,)) for _ in range(2)]
        + [dma((2 * GROUPS,)) for _ in range(2)]
        + [dma((2,)) for _ in range(2)]
        + [dma((2 * GROUPS,)) for _ in range(2)],
        compiler_params=pltpu.CompilerParams(
            collective_id=0, has_side_effects=True, vmem_limit_bytes=64400 * 1024
        ),
    )(
        tokens, norm_gain.reshape(1, features), route_ids.T, route_weights.T,
        w_gate[0], w_up[0], w_down[0],
    )


def solution(mesh):
    sizes = mesh.shape

    def per_device(tokens, norm_gain, route_ids, route_weights, w_gate, w_up, w_down):
        arguments = (tokens, norm_gain, route_ids, route_weights, w_gate, w_up, w_down)
        members = sizes["ep"] * w_gate.shape[0] // GROUPS
        paired = members == route_ids.shape[1] == sizes["grp"] == sizes["tp"] == 2
        if paired and w_gate.shape[0] == 1:
            return group_layer(members, *arguments)
        return general_layer(*arguments)

    in_specs = (
        P(("grp", "ep", "tp"), None),
        P(),
        P(("grp", "ep", "tp"), None),
        P(("grp", "ep", "tp"), None),
        P("ep", None, "tp"),
        P("ep", None, "tp"),
        P("ep", "tp", None),
    )
    out_specs = P(("grp", "ep", "tp"), None)
    return jax.shard_map(
        per_device, mesh=mesh, in_specs=in_specs, out_specs=out_specs, check_vma=False
    )
```

time: 97.1 us -> 113 us (1.16)
  the two profiles are of different devices: /device:TPU:8 before, /device:TPU:0 now
where the time goes in v2:
time: 113 us
  Pallas kernels  112 us (99%)
    pallas_call x1, Pallas kernels, group_layer(): pl.pallas_call(functools.partial(group_kernel, members, parts, halves), o...  112 us

profile of v2, /device:TPU:0, one launch (start us, length us, event | category | flops | bytes accessed | tf_op | source)
XLA Modules:
  0.0 113.2 jit_solution(9853100639905647029)
XLA Ops:
  0.0 112.2 %shard_map.73 = bf16[256,2048]{1,0:T(8,128)(2,1)S(1)} custom-call(bf16[256,2048]{1,0:T(8,128)(2,1)} %tokens.1, f32[1,2048]{1,0:T(1,128)} %bitcast.9, s32[2,256]{1,0:T(2,128)} %bitcast.10, f32[2,256]{1,0:T(2,128)} %bitcast.11, bf16[2048,256]{1,0:T(8,128)(2,1)} %bitcast.6, bf16[2048,256]{1,0:T(8,128)(2,1)} %bitcast.7, bf16[256,2048]{1,0:T(8,128)(2,1)} %bitcast.8), custom_call_target="tpu_custom_call" | custom-call | tf_op jit(solution)/shard_map/pallas_call | solution.py:512
  112.2 1.0 copy.9

commit v3 on v1

--- a/solution.py
+++ b/solution.py
@@ -8,7 +8,6 @@
 from jax.sharding import PartitionSpec as P
 
 GROUPS = 4
-EARLY = 1
 SPLIT = 4
 MESH = pl.DeviceIdType.MESH
 
@@ -65,8 +64,8 @@
     tokens, gain_in, ids_in, weights_in, w_gate, w_up, w_down, out,
     gain, ids, weights, raw, ready, summed, place, sent, taken, scales, scales_in, answers, returned,
     gate_all, up_all, down_all, hidden,
-    raw_sem, small_sems, own_sems, twin_s, twin_r, peer_s, peer_r, part_s, part_r,
-    near_s, near_r, far_s, far_r, row_s, row_r, scale_s, scale_r, back_s, back_r,
+    raw_sem, small_sems, peer_s, peer_r, part_s, part_r, twin_s, twin_r,
+    row_s, row_r, scale_s, scale_r, back_s, back_r,
 ):
     part, position, half = lax.axis_index("grp"), lax.axis_index("ep"), lax.axis_index("tp")
     level, member = position // members, position % members
@@ -118,31 +117,31 @@
         tensor, window = span(index, part)
         return remote(
             sources[tensor].at[window], stores[tensor].at[mine, window],
-            peer_s.at[index], peer_r.at[index], peer,
+            peer_s.at[tensor], peer_r.at[index], peer,
         )
 
     def spread_copy(index, which, send, recv, device):
         tensor, window = span(index, which)
         block = stores[tensor].at[theirs, window]
-        return remote(block, block, send.at[index], recv.at[index], device)
-
-    peer_copies = [peer_copy(index) for index in range(len(pieces))]
-    part_copies = [spread_copy(i, part, part_s, part_r, other_part) for i in range(len(pieces))]
-    near_copies = [spread_copy(i, part, near_s, near_r, twin) for i in range(len(pieces))]
-    far_copies = [
-        spread_copy(i, parts - 1 - part, far_s, far_r, twin) for i in range(len(pieces))
-    ]
-    own_copies, twin_copies = [], []
+        return remote(block, block, send.at[tensor], recv, device)
+
+    indices = range(len(pieces))
+    peer_copies = [peer_copy(index) for index in indices]
+    part_copies = [spread_copy(i, part, part_s, part_r.at[i], other_part) for i in indices]
+    near_copies = [spread_copy(i, part, twin_s, twin_r.at[i % 3], twin) for i in indices]
+    far_copies = [spread_copy(i, parts - 1 - part, twin_s, twin_r.at[i % 3], twin) for i in indices]
+    own_copies, twin_copies, twin_all, half_all = [], [], [], []
     for tensor in range(3):
-        own_copies.append(
-            pltpu.make_async_copy(sources[tensor], stores[tensor].at[mine], own_sems.at[tensor])
-        )
+        own = stores[tensor].at[mine]
+        own_copies.append(pltpu.make_async_copy(sources[tensor], own, small_sems.at[tensor]))
         twin_copies.append(
-            remote(
-                sources[tensor], stores[tensor].at[mine],
-                twin_s.at[tensor], twin_r.at[tensor], twin,
-            )
-        )
+            remote(sources[tensor], own, twin_s.at[tensor], twin_r.at[tensor], twin)
+        )
+        both = stores[tensor].at[0:2]
+        twin_all.append(remote(both, both, twin_s.at[tensor], twin_r.at[tensor], twin))
+        piece = stores[tensor].at[0, 0 : sources[tensor].shape[0] // parts]
+        for send, device in ((peer_s, peer), (part_s, other_part)):
+            half_all.append(remote(piece, piece, send.at[tensor], peer_r.at[0], device))
     for copy in small_copies:
         copy.wait()
     first = ids[0:1, :]
@@ -170,14 +169,28 @@
     middle = rest.astype(jnp.bfloat16)
     low = (rest - middle.astype(jnp.float32)).astype(jnp.bfloat16)
 
+    tile = features // GROUPS
+    order = (2, 1, 3, 0)
+    tiles = [slice(begin, begin + tile) for begin in range(0, features, tile)]
     row_copies, scale_copies, back_copies = {}, {}, {}
     slot_iota = lax.broadcasted_iota(jnp.int32, (slots, rows), 0)
-    order = (2, 1, 3, 0)
     for k in (1, 2, 3):
-        row_copies[k] = remote(sent.at[k], taken.at[k], row_s.at[k], row_r.at[k], level_of(k))
+        row_copies[k] = remote(
+            sent.at[k], taken.at[k], row_s, row_r.at[k - 1], level_of(k)
+        )
         scale_copies[k] = remote(
-            scales.at[k], scales_in.at[k], scale_s.at[k], scale_r.at[k], level_of(k)
-        )
+            scales.at[k, :members], scales_in.at[k, :members],
+            scale_s, scale_r.at[k - 1], level_of(k),
+        )
+
+        cut = tiles if k == order[-2] else [slice(0, features)]
+        back_copies[k] = [
+            remote(
+                answers.at[k, :, window], returned.at[k, :, window],
+                back_s, back_r.at[k - 1 + t], level_of(k),
+            )
+            for t, window in enumerate(cut)
+        ]
 
     def pack(k):
         key = jnp.where(group_row == (level ^ k), slot_row, -1)
@@ -197,15 +210,14 @@
         )
 
     raw_copy.wait()
-    for k in order[:EARLY]:
-        pack(k)
+    pack(order[0])
     pl.semaphore_wait(barrier, len(neighbours))
     for k in order:
-        if k not in order[:EARLY]:
+        if k != order[0]:
             pack(k)
         if k:
+            scale_copies[k].start()
             row_copies[k].start()
-            scale_copies[k].start()
         if k == order[0]:
             for copy in peer_copies + own_copies + twin_copies:
                 copy.start()
@@ -224,7 +236,6 @@
     diagonal = lax.broadcasted_iota(jnp.int32, (slots, slots), 0) == lax.broadcasted_iota(
         jnp.int32, (slots, slots), 1
     )
-    tile = features // GROUPS
 
     strip = 32
 
@@ -253,8 +264,7 @@
             ).astype(jnp.bfloat16)
 
     def narrow(k):
-        for column in range(features // tile):
-            window = slice(column * tile, (column + 1) * tile)
+        for column, window in enumerate(tiles):
             total = jnp.zeros((slots, tile), jnp.float32)
             for block in range(members * halves):
                 total += jnp.dot(
@@ -264,12 +274,14 @@
                 )
             if k:
                 answers[k, :, window] = total.astype(jnp.bfloat16)
+                if k == order[-2]:
+                    back_copies[k][column].start()
             else:
                 returned[0, :, window] = total.astype(jnp.bfloat16)
 
     for copy in own_copies:
         copy.wait()
-    for copy in twin_copies:
+    for copy in twin_all:
         copy.wait_recv()
     for k in order:
         if k:
@@ -277,16 +289,10 @@
             scale_copies[k].wait_recv()
         norm(k)
         widen(k, member)
-        if k == order[0]:
-            for copy in near_copies + far_copies:
-                copy.wait_recv()
         widen(k, members - 1 - member)
         narrow(k)
-        if k:
-            back_copies[k] = remote(
-                answers.at[k], returned.at[k], back_s.at[k], back_r.at[k], level_of(k)
-            )
-            back_copies[k].start()
+        if k and k != order[-2]:
+            back_copies[k][0].start()
 
     def unpack(k, window):
         return lax.dot_general(
@@ -294,24 +300,23 @@
             (((0,), (0,)), ((), ())), preferred_element_type=jnp.float32,
         )
 
-    tiles = [slice(start, start + tile) for start in range(0, features, tile)]
     for window in tiles:
         summed[:, window] = unpack(0, window)
     for k in order[:-1]:
-        back_copies[k].wait_recv()
-        for window in tiles:
+        for t, window in enumerate(tiles):
+            if t < len(back_copies[k]):
+                back_copies[k][t].wait_recv()
             total = summed[:, window] + unpack(k, window)
             if k == order[-2]:
                 out[:, window] = total.astype(jnp.bfloat16)
             else:
                 summed[:, window] = total
 
-    for copy in peer_copies + part_copies + near_copies + far_copies + twin_copies:
+    for copy in half_all + twin_all:
         copy.wait_send()
-    for k in (1, 2, 3):
-        row_copies[k].wait_send()
-        scale_copies[k].wait_send()
-        back_copies[k].wait_send()
+    for buffer, sem in ((sent, row_s), (scales, scale_s), (answers, back_s)):
+        used = buffer.at[1:GROUPS] if sem is not scale_s else buffer.at[1:GROUPS, :members]
+        remote(used, used, sem, back_r.at[0], twin).wait_send()
 
 
 def group_layer(members, tokens, norm_gain, route_ids, route_weights, w_gate, w_up, w_down):
@@ -346,10 +351,9 @@
             pltpu.VMEM((blocks, features, width), bf16),
             pltpu.VMEM((blocks, width, features), bf16),
             pltpu.VMEM((slots, blocks * width), bf16),
-            dma, dma((3,)), dma((3,)), dma((3,)), dma((3,)),
-        ]
-        + [dma((copies,)) for _ in range(8)]
-        + [dma((GROUPS,)) for _ in range(6)],
+            dma, dma((3,)), dma((3,)), dma((copies,)), dma((3,)), dma((copies,)),
+            dma((3,)), dma((3,)), dma, dma((3,)), dma, dma((3,)), dma, dma((6,)),
+        ],
         compiler_params=pltpu.CompilerParams(
             collective_id=0, has_side_effects=True, vmem_limit_bytes=64400 * 1024
         ),

time: 97.1 us -> 95.8 us (0.987)
  Pallas kernels: 95.9 us -> 94.2 us
    pallas_call x1, Pallas kernels: 95.9 us -> 94.2 us  [group_layer(): pl.pallas_call(functools.partial(group_kernel, members, parts, halves), o...]
where the time goes in v3:
time: 95.8 us; the launch traced here: 95.2 us
  Pallas kernels  94.2 us (98%)
  local copies, waits for them, and re-layouts  0.97 us (1%)
    pallas_call x1, Pallas kernels, group_layer(): pl.pallas_call(functools.partial(group_kernel, members, parts, halves), o...  94.2 us

profile of v3, /device:TPU:8, one launch (start us, length us, event | category | flops | bytes accessed | tf_op | source)
XLA Modules:
  0.0 95.2 jit_solution(8498211555719843404)
XLA Ops:
  0.0 94.2 %shard_map.73 = bf16[256,2048]{1,0:T(8,128)(2,1)S(1)} custom-call(bf16[256,2048]{1,0:T(8,128)(2,1)} %tokens.1, f32[1,2048]{1,0:T(1,128)} %bitcast.9, s32[2,256]{1,0:T(2,128)} %bitcast.10, f32[2,256]{1,0:T(2,128)} %bitcast.11, bf16[2048,256]{1,0:T(8,128)(2,1)} %bitcast.6, bf16[2048,256]{1,0:T(8,128)(2,1)} %bitcast.7, bf16[256,2048]{1,0:T(8,128)(2,1)} %bitcast.8), custom_call_target="tpu_custom_call" | custom-call | tf_op jit(solution)/shard_map/pallas_call | solution.py:331
  94.2 1.0 %copy.9 = bf16[256,2048]{1,0:T(8,128)(2,1)} copy(bf16[256,2048]{1,0:T(8,128)(2,1)S(1)} %shard_map.73) | data formatting | bytes 2097152

commit v4 on v3

--- a/solution.py
+++ b/solution.py
@@ -62,10 +62,11 @@
 def group_kernel(
     members, parts, halves,
     tokens, gain_in, ids_in, weights_in, w_gate, w_up, w_down, out,
-    gain, ids, weights, raw, ready, summed, place, sent, taken, scales, scales_in, answers, returned,
+    gain, ids, weights, raw, ready, summed, place, sent, taken, scales, scales_in, answers,
+    returned,
     gate_all, up_all, down_all, hidden,
-    raw_sem, small_sems, peer_s, peer_r, part_s, part_r, twin_s, twin_r,
-    row_s, row_r, scale_s, scale_r, back_s, back_r,
+    raw_sems, small_sems, peer_r, part_r, twin_r, weight_s, row_s, row_r, scale_s, scale_r,
+    back_s, back_r,
 ):
     part, position, half = lax.axis_index("grp"), lax.axis_index("ep"), lax.axis_index("tp")
     level, member = position // members, position % members
@@ -83,12 +84,18 @@
     neighbours = [level_of(k) for k in range(GROUPS - 1, 0, -1)] + [peer, other_part, twin]
     for device in neighbours:
         pl.semaphore_signal(barrier, inc=1, device_id=device, device_id_type=MESH)
+    tile = features // GROUPS
+    tiles = [slice(begin, begin + tile) for begin in range(0, features, tile)]
     small_copies = [
         pltpu.make_async_copy(src, dst, small_sems.at[i])
         for i, (src, dst) in enumerate(((ids_in, ids), (weights_in, weights), (gain_in, gain)))
     ]
-    raw_copy = pltpu.make_async_copy(tokens, raw, raw_sem)
-    for copy in small_copies + [raw_copy]:
+    raw_copies = []
+    for i, window in enumerate((tiles[0], slice(tile, features))):
+        raw_copies.append(
+            pltpu.make_async_copy(tokens.at[:, window], raw.at[:, window], raw_sems.at[i])
+        )
+    for copy in small_copies[:1] + raw_copies + small_copies[1:]:
         copy.start()
 
     sources = (w_gate, w_up, w_down)
@@ -117,70 +124,56 @@
         tensor, window = span(index, part)
         return remote(
             sources[tensor].at[window], stores[tensor].at[mine, window],
-            peer_s.at[tensor], peer_r.at[index], peer,
-        )
-
-    def spread_copy(index, which, send, recv, device):
+            weight_s.at[tensor], peer_r.at[index], peer,
+        )
+
+    def spread_copy(index, which, recv, device):
         tensor, window = span(index, which)
         block = stores[tensor].at[theirs, window]
-        return remote(block, block, send.at[tensor], recv, device)
+        return remote(block, block, weight_s.at[tensor], recv, device)
 
     indices = range(len(pieces))
     peer_copies = [peer_copy(index) for index in indices]
-    part_copies = [spread_copy(i, part, part_s, part_r.at[i], other_part) for i in indices]
-    near_copies = [spread_copy(i, part, twin_s, twin_r.at[i % 3], twin) for i in indices]
-    far_copies = [spread_copy(i, parts - 1 - part, twin_s, twin_r.at[i % 3], twin) for i in indices]
-    own_copies, twin_copies, twin_all, half_all = [], [], [], []
+    part_copies = [spread_copy(i, part, part_r.at[i], other_part) for i in indices]
+    near_copies = [spread_copy(i, part, twin_r.at[i % 3], twin) for i in indices]
+    far_copies = [spread_copy(i, parts - 1 - part, twin_r.at[i % 3], twin) for i in indices]
+    own_copies, twin_copies, twin_all, sent_all = [], [], [], []
     for tensor in range(3):
         own = stores[tensor].at[mine]
         own_copies.append(pltpu.make_async_copy(sources[tensor], own, small_sems.at[tensor]))
         twin_copies.append(
-            remote(sources[tensor], own, twin_s.at[tensor], twin_r.at[tensor], twin)
-        )
-        both = stores[tensor].at[0:2]
-        twin_all.append(remote(both, both, twin_s.at[tensor], twin_r.at[tensor], twin))
-        piece = stores[tensor].at[0, 0 : sources[tensor].shape[0] // parts]
-        for send, device in ((peer_s, peer), (part_s, other_part)):
-            half_all.append(remote(piece, piece, send.at[tensor], peer_r.at[0], device))
-    for copy in small_copies:
-        copy.wait()
-    first = ids[0:1, :]
-    group_row = first // members
+            remote(sources[tensor], own, weight_s.at[tensor], twin_r.at[tensor], twin)
+        )
+        for blocks, waits in ((2, twin_all), (3, sent_all)):
+            span_all = stores[tensor].at[0:blocks]
+            waits.append(
+                remote(span_all, span_all, weight_s.at[tensor], twin_r.at[tensor], twin)
+            )
     lane = lax.broadcasted_iota(jnp.int32, (8, rows), 0)
-    mask = (jnp.broadcast_to(group_row, (8, rows)) == lane).astype(jnp.float32)
     before = (
         lax.broadcasted_iota(jnp.int32, (rows, rows), 0)
         < lax.broadcasted_iota(jnp.int32, (rows, rows), 1)
-    ).astype(jnp.float32)
-    ranks = jnp.dot(
-        mask.astype(jnp.bfloat16), before.astype(jnp.bfloat16),
-        preferred_element_type=jnp.float32,
-    )
+    ).astype(jnp.float32).astype(jnp.bfloat16)
+    slot_iota = lax.broadcasted_iota(jnp.int32, (slots, rows), 0)
+    small_copies[0].wait()
+    first = ids[0:1, :]
+    group_row = first // members
+    mask = (jnp.broadcast_to(group_row, (8, rows)) == lane).astype(jnp.float32)
+    ranks = jnp.dot(mask.astype(jnp.bfloat16), before, preferred_element_type=jnp.float32)
     slot_row = jnp.sum(ranks * mask, axis=0, keepdims=True).astype(jnp.int32)
-    shares = jnp.zeros((8, rows), jnp.float32)
-    for column in range(top_count):
-        offset = ids[column : column + 1, :] - group_row * members
-        chosen = jnp.broadcast_to(offset, (8, rows)) == lane
-        shares = shares + jnp.where(
-            chosen, jnp.broadcast_to(weights[column : column + 1, :], (8, rows)), 0.0
-        )
-    high = shares.astype(jnp.bfloat16)
-    rest = shares - high.astype(jnp.float32)
-    middle = rest.astype(jnp.bfloat16)
-    low = (rest - middle.astype(jnp.float32)).astype(jnp.bfloat16)
-
-    tile = features // GROUPS
     order = (2, 1, 3, 0)
-    tiles = [slice(begin, begin + tile) for begin in range(0, features, tile)]
     row_copies, scale_copies, back_copies = {}, {}, {}
-    slot_iota = lax.broadcasted_iota(jnp.int32, (slots, rows), 0)
     for k in (1, 2, 3):
-        row_copies[k] = remote(
-            sent.at[k], taken.at[k], row_s, row_r.at[k - 1], level_of(k)
-        )
+        row_copies[k] = [
+            remote(
+                sent.at[k, :, window], taken.at[k, :, window],
+                row_s, row_r.at[k - 1], level_of(k),
+            )
+            for window in (tiles if k == order[0] else [slice(0, features)])
+        ]
         scale_copies[k] = remote(
             scales.at[k, :members], scales_in.at[k, :members],
-            scale_s, scale_r.at[k - 1], level_of(k),
+            scale_s, scale_r, level_of(k),
         )
 
         cut = tiles if k == order[-2] else [slice(0, features)]
@@ -192,35 +185,62 @@
             for t, window in enumerate(cut)
         ]
 
-    def pack(k):
+    def find(k):
         key = jnp.where(group_row == (level ^ k), slot_row, -1)
         spots = (jnp.broadcast_to(key, (slots, rows)) == slot_iota).astype(jnp.float32)
         spots = spots.astype(jnp.bfloat16)
         place[k * slots : (k + 1) * slots, :] = spots
-        lanes = sum(
+        return spots
+
+    def pack(k, spots, window):
+        packed = taken if k == 0 else sent
+        packed[k, :, window] = jnp.dot(
+            spots, raw[:, window], preferred_element_type=jnp.float32
+        ).astype(jnp.bfloat16)
+
+    early = order[0]
+    spots = find(early)
+    raw_copies[0].wait()
+    pack(early, spots, tiles[0])
+    pl.semaphore_wait(barrier, len(neighbours))
+    row_copies[early][0].start()
+    for copy in peer_copies:
+        copy.start()
+    raw_copies[1].wait()
+    for window, copy in zip(tiles[1:], row_copies[early][1:]):
+        pack(early, spots, window)
+        copy.start()
+    for copy in small_copies[1:]:
+        copy.wait()
+    found = {k: find(k) for k in order[1:]}
+    shares = jnp.zeros((8, rows), jnp.float32)
+    for column in range(top_count):
+        offset = ids[column : column + 1, :] - group_row * members
+        chosen = jnp.broadcast_to(offset, (8, rows)) == lane
+        shares = shares + jnp.where(
+            chosen, jnp.broadcast_to(weights[column : column + 1, :], (8, rows)), 0.0
+        )
+    high = shares.astype(jnp.bfloat16)
+    rest = shares - high.astype(jnp.float32)
+    middle = rest.astype(jnp.bfloat16)
+    low = (rest - middle.astype(jnp.float32)).astype(jnp.bfloat16)
+    for k in order:
+        (scales if k else scales_in)[k] = sum(
             lax.dot_general(
-                piece, spots, (((1,), (1,)), ((), ())), preferred_element_type=jnp.float32
+                piece, place[k * slots : (k + 1) * slots, :], (((1,), (1,)), ((), ())),
+                preferred_element_type=jnp.float32,
             )
             for piece in (high, middle, low)
         )
-        packed = taken if k == 0 else sent
-        (scales_in if k == 0 else scales)[k] = lanes
-        packed[k] = jnp.dot(spots, raw[...], preferred_element_type=jnp.float32).astype(
-            jnp.bfloat16
-        )
-
-    raw_copy.wait()
-    pack(order[0])
-    pl.semaphore_wait(barrier, len(neighbours))
-    for k in order:
-        if k != order[0]:
-            pack(k)
         if k:
             scale_copies[k].start()
-            row_copies[k].start()
-        if k == order[0]:
-            for copy in peer_copies + own_copies + twin_copies:
-                copy.start()
+
+    for k in order[1:]:
+        pack(k, found[k], slice(0, features))
+        if k:
+            row_copies[k][0].start()
+    for copy in own_copies + twin_copies:
+        copy.start()
 
     for index in range(len(pieces)):
         peer_copies[index].wait_recv()
@@ -281,12 +301,13 @@
 
     for copy in own_copies:
         copy.wait()
-    for copy in twin_all:
+    scale_all = scales.at[1:GROUPS, :members]
+    scale_all = remote(scale_all, scale_all, scale_s, scale_r, twin)
+    for copy in twin_all + [scale_all]:
         copy.wait_recv()
     for k in order:
         if k:
-            row_copies[k].wait_recv()
-            scale_copies[k].wait_recv()
+            remote(sent.at[k], taken.at[k], row_s, row_r.at[k - 1], twin).wait_recv()
         norm(k)
         widen(k, member)
         widen(k, members - 1 - member)
@@ -312,11 +333,11 @@
             else:
                 summed[:, window] = total
 
-    for copy in half_all + twin_all:
+    for buffer, sem in ((sent, row_s), (answers, back_s)):
+        flows = buffer.at[1:GROUPS]
+        sent_all.append(remote(flows, flows, sem, back_r.at[0], twin))
+    for copy in sent_all + [scale_all]:
         copy.wait_send()
-    for buffer, sem in ((sent, row_s), (scales, scale_s), (answers, back_s)):
-        used = buffer.at[1:GROUPS] if sem is not scale_s else buffer.at[1:GROUPS, :members]
-        remote(used, used, sem, back_r.at[0], twin).wait_send()
 
 
 def group_layer(members, tokens, norm_gain, route_ids, route_weights, w_gate, w_up, w_down):
@@ -351,8 +372,8 @@
             pltpu.VMEM((blocks, features, width), bf16),
             pltpu.VMEM((blocks, width, features), bf16),
             pltpu.VMEM((slots, blocks * width), bf16),
-            dma, dma((3,)), dma((3,)), dma((copies,)), dma((3,)), dma((copies,)),
-            dma((3,)), dma((3,)), dma, dma((3,)), dma, dma((3,)), dma, dma((6,)),
+            dma((2,)), dma((3,)), dma((copies,)), dma((copies,)), dma((3,)), dma((3,)),
+            dma, dma((3,)), dma, dma, dma, dma((6,)),
         ],
         compiler_params=pltpu.CompilerParams(
             collective_id=0, has_side_effects=True, vmem_limit_bytes=64400 * 1024

time: 95.8 us -> 95.6 us (level)
  no operation moved by 1% of the time
where the time goes in v4:
time: 95.6 us; the launch traced here: 94.7 us
  Pallas kernels  93.7 us (98%)
  local copies, waits for them, and re-layouts  0.97 us (1%)
    pallas_call x1, Pallas kernels, group_layer(): pl.pallas_call(functools.partial(group_kernel, members, parts, halves), o...  93.7 us

profile of v4, /device:TPU:8, one launch (start us, length us, event | category | flops | bytes accessed | tf_op | source)
XLA Modules:
  0.0 94.7 jit_solution(10443940282454432042)
XLA Ops:
  0.0 93.7 %shard_map.73 = bf16[256,2048]{1,0:T(8,128)(2,1)S(1)} custom-call(bf16[256,2048]{1,0:T(8,128)(2,1)} %tokens.1, f32[1,2048]{1,0:T(1,128)} %bitcast.9, s32[2,256]{1,0:T(2,128)} %bitcast.10, f32[2,256]{1,0:T(2,128)} %bitcast.11, bf16[2048,256]{1,0:T(8,128)(2,1)} %bitcast.6, bf16[2048,256]{1,0:T(8,128)(2,1)} %bitcast.7, bf16[256,2048]{1,0:T(8,128)(2,1)} %bitcast.8), custom_call_target="tpu_custom_call" | custom-call | tf_op jit(solution)/shard_map/pallas_call | solution.py:352
  93.7 1.0 %copy.9 = bf16[256,2048]{1,0:T(8,128)(2,1)} copy(bf16[256,2048]{1,0:T(8,128)(2,1)S(1)} %shard_map.73) | data formatting | bytes 2097152

commit v5 on v2

--- a/solution.py
+++ b/solution.py
@@ -9,7 +9,9 @@
 
 GROUPS = 4
 SPLIT = 4
-SWAP_AT = 11
+HELD = 0
+LATE = 7
+FIRST = True
 MESH = pl.DeviceIdType.MESH
 
 
@@ -65,11 +67,9 @@
     tokens, gain_in, ids_in, weights_in, w_gate, w_up, w_down, out,
     gain, ids, weights, raw, ready, summed, place, sent, taken, scales, scales_in, answers,
     returned, gate_all, up_all, down_all, hidden,
-    own_gate, own_up, own_down, peer_rows, peer_scales, partial, parts_out, parts_in,
-    raw_sem, small_sems, own_sems, twin_s, twin_r, peer_s, peer_r, part_s, part_r,
-    near_s, near_r, far_s, far_r, guest_s, guest_r, cross_s, cross_r,
-    gnear_s, gnear_r, gfar_s, gfar_r, row_s, row_r, scale_s, scale_r, back_s, back_r,
-    swap_s, swap_r, note_s, note_r, half_s, half_r,
+    own_gate, own_up, own_down, extra, extra_scales, partial, parts_out, parts_in,
+    raw_sem, small_sems, peer_r, part_r, twin_r, own_r, weight_s, row_s, swap_s, scale_s,
+    note_s, back_s, half_s, row_r, extra_r, scale_r, note_r, back_r, half_r,
 ):
     part, position, half = lax.axis_index("grp"), lax.axis_index("ep"), lax.axis_index("tp")
     level, member = position // members, position % members
@@ -80,6 +80,7 @@
     peer = {"ep": level * members + (members - 1 - member)}
     other_part = {"grp": parts - 1 - part}
     twin = {"tp": halves - 1 - half}
+    slant = {"ep": (level ^ 1) * members + (members - 1 - member)}
 
     def level_of(k):
         return {"ep": (level ^ k) * members + member}
@@ -87,7 +88,7 @@
     on_inner, on_outer = pl.when(inner == 1), pl.when(inner == 0)
 
     barrier = pltpu.get_barrier_semaphore()
-    neighbours = [level_of(k) for k in range(GROUPS - 1, 0, -1)] + [peer, other_part, twin]
+    neighbours = [level_of(k) for k in range(GROUPS - 1, 0, -1)] + [slant, peer, other_part, twin]
     for device in neighbours:
         pl.semaphore_signal(barrier, inc=1, device_id=device, device_id_type=MESH)
     small_copies = [
@@ -120,48 +121,55 @@
         size = sources[tensor].shape[0] // (parts * SPLIT)
         return pl.ds(pl.multiple_of((which * SPLIT + step) * size, size), size)
 
-    def first_copies(send, recv, device):
+    def first_copies(device):
         copies = []
         for i, piece in enumerate(pieces):
             window = window_of(piece, part)
             copies.append(remote(
                 sources[piece[0]].at[window], stores[piece[0]].at[mine, window],
-                send.at[i], recv.at[i], device,
+                weight_s.at[piece[0]], peer_r.at[i], device,
             ))
         return copies
 
-    def spread_copies(block, which, send, recv, device):
+    def spread_copies(block, which, device):
         copies = []
         for i, piece in enumerate(pieces):
             held = stores[piece[0]].at[block, window_of(piece, which)]
-            copies.append(remote(held, held, send.at[i], recv.at[i], device))
+            recv = twin_r.at[piece[0]] if device is twin else part_r.at[i]
+            copies.append(remote(held, held, weight_s.at[piece[0]], recv, device))
         return copies
 
     other = parts - 1 - part
-    peer_copies = first_copies(peer_s, peer_r, peer)
-    relay_copies = spread_copies(mine, part, peer_s, peer_r, peer)
-    part_copies = spread_copies(theirs, part, part_s, part_r, other_part)
-    near_copies = spread_copies(theirs, part, near_s, near_r, twin)
-    far_copies = spread_copies(theirs, other, far_s, far_r, twin)
-    guest_copies = first_copies(guest_s, guest_r, level_of(GROUPS - 1))
-    cross_copies = spread_copies(mine, part, cross_s, cross_r, other_part)
-    gnear_copies = spread_copies(mine, part, gnear_s, gnear_r, twin)
-    gfar_copies = spread_copies(mine, other, gfar_s, gfar_r, twin)
-
-    def home_copies(targets, block):
+    peer_copies = first_copies(peer)
+    part_copies = spread_copies(theirs, part, other_part)
+    near_copies = spread_copies(theirs, part, twin)
+    far_copies = spread_copies(theirs, other, twin)
+    guest_copies = first_copies(level_of(GROUPS - 1))
+    cross_copies = spread_copies(mine, part, other_part)
+    gnear_copies = spread_copies(mine, part, twin)
+    gfar_copies = spread_copies(mine, other, twin)
+
+    def home_copies(targets, block, recv):
         copies, twins = [], []
         for tensor in range(3):
             target = targets[tensor].at[block]
             copies.append(
-                pltpu.make_async_copy(sources[tensor], target, own_sems.at[tensor])
+                pltpu.make_async_copy(sources[tensor], target, small_sems.at[tensor])
             )
             twins.append(
-                remote(sources[tensor], target, twin_s.at[tensor], twin_r.at[tensor], twin)
+                remote(sources[tensor], target, weight_s.at[tensor], recv.at[tensor], twin)
             )
         return copies, twins
 
-    group_copies, group_twins = home_copies(stores, mine)
-    own_copies, own_twins = home_copies(own_stores, half)
+    def block_waits(count):
+        waits = []
+        for tensor in range(3):
+            held = stores[tensor].at[0:count]
+            waits.append(remote(held, held, weight_s.at[tensor], twin_r.at[tensor], twin))
+        return waits
+
+    group_copies, group_twins = home_copies(stores, mine, twin_r)
+    own_copies, own_twins = home_copies(own_stores, half, own_r)
     row_to = {1: level_of(1), 2: level_of(1 + inner), 3: level_of(3)}
     back_to = {1: level_of(1), 2: level_of(2 - inner), 3: level_of(3)}
     tile = features // GROUPS
@@ -169,27 +177,47 @@
 
     def tiled_copies(src, dst, send, recv, base, device):
         return [
-            remote(
-                src.at[:, window], dst.at[:, window],
-                send.at[base * GROUPS + t], recv.at[base * GROUPS + t], device,
-            )
+            remote(src.at[:, window], dst.at[:, window], send, recv.at[base + t], device)
             for t, window in enumerate(tiles)
         ]
 
-    row_copies, scale_copies, back_copies = {}, {}, {}
+    row_copies, scale_copies = {}, {}
     for k in (1, 2, 3):
-        row_copies[k] = tiled_copies(sent.at[k], taken.at[k], row_s, row_r, k, row_to[k])
+        row_copies[k] = remote(sent.at[k], taken.at[k], row_s, row_r.at[k - 1], row_to[k])
         scale_copies[k] = remote(
-            scales.at[k], scales_in.at[k], scale_s.at[k], scale_r.at[k], row_to[k]
-        )
-        back_copies[k] = tiled_copies(answers.at[k], returned.at[k], back_s, back_r, k, back_to[k])
-    swap_copies, note_copies, half_copies = [], [], []
-    for j, k in enumerate((1, 0)):
-        swap_copies.append(tiled_copies(taken.at[k], peer_rows.at[j], swap_s, swap_r, j, peer))
-        note_copies.append(
-            remote(scales_in.at[k], peer_scales.at[j], note_s.at[j], note_r.at[j], peer)
-        )
-        half_copies.append(tiled_copies(parts_out.at[j], parts_in.at[j], half_s, half_r, j, peer))
+            scales.at[k, :members], scales_in.at[k, :members],
+            scale_s, scale_r.at[k - 1], row_to[k],
+        )
+    slant_rows = remote(sent.at[1], extra.at[0], row_s, extra_r.at[0], slant)
+    slant_scales = remote(
+        scales.at[1, :members], extra_scales.at[0, :members], scale_s, note_r.at[0], slant
+    )
+    back_copies = {
+        1: [remote(answers.at[1], returned.at[1], back_s, back_r.at[0], back_to[1])],
+        2: tiled_copies(answers.at[2], returned.at[2], back_s, back_r, 1, back_to[2]),
+        3: tiled_copies(answers.at[3], returned.at[3], back_s, back_r, 5, back_to[3]),
+    }
+    swap_copies, note_copies, half_copies = {}, {}, {}
+    for j, (buffer, source, k) in enumerate(
+        ((taken, scales_in, 0), (taken, scales_in, 2), (sent, scales, 3)), 1
+    ):
+        swap_copies[j] = remote(buffer.at[k], extra.at[j], swap_s, extra_r.at[j], peer)
+        note_copies[j] = remote(
+            source.at[k, :members], extra_scales.at[j, :members], note_s, note_r.at[j], peer
+        )
+    for j, device in ((0, slant), (3, peer)):
+        half_copies[j] = [
+            remote(parts_out.at[j], parts_in.at[j], half_s, half_r.at[j], device)
+        ]
+    middle = features // 2
+    half_copies[1] = [
+        remote(
+            parts_out.at[1, :, window], parts_in.at[1, :, window],
+            half_s, half_r.at[1 + t], peer,
+        )
+        for t, window in enumerate((slice(0, middle), slice(middle, features)))
+    ]
+    half_copies[2] = tiled_copies(parts_out.at[2], parts_in.at[2], half_s, half_r, 4, peer)
 
     for copy in small_copies:
         copy.wait()
@@ -248,12 +276,16 @@
         for copy in copies:
             copy.wait_send()
 
+    def swap(j):
+        note_copies[j].start()
+        swap_copies[j].start()
+
     def send(k):
         scale_copies[k].start()
-        start(row_copies[k])
+        row_copies[k].start()
 
     def arrive(k):
-        land(row_copies[k] + [scale_copies[k]])
+        land([scale_copies[k], row_copies[k]])
 
     raw_copy.wait()
     pack(1)
@@ -267,12 +299,15 @@
 
     @on_outer
     def _():
+        slant_scales.start()
+        slant_rows.start()
         start(peer_copies)
 
     pack(0)
 
     @on_inner
     def _():
+        swap(1)
         start(own_copies + own_twins)
 
     @on_outer
@@ -338,43 +373,48 @@
             window, total = narrow(base, slots * len(targets), group_down, column)
             for j, (target, copies) in enumerate(targets):
                 target[:, window] = total[j * slots : (j + 1) * slots].astype(jnp.bfloat16)
-                if copies:
+                if copies and column < len(copies):
                     copies[column].start()
 
-    def whole(pair, base):
-        for j, k in enumerate(pair):
-            norm(taken.at[k], base + j * slots)
+    def whole(ks, held=0):
+        for j, k in enumerate(ks):
+            norm(taken.at[k], j * slots)
         for owner in range(members):
             for side in range(halves):
-                widen_group(base, [scales_in.at[k] for k in pair], owner, side)
-        narrow_group(
-            base, [((answers if k else returned).at[k], back_copies.get(k)) for k in pair]
-        )
-
-    def divided(j, k):
-        base = 2 * slots * j
-        norm(peer_rows.at[j], base)
-        norm(taken.at[k], base + slots)
+                widen_group(0, [scales_in.at[k] for k in ks], owner, side)
+        targets = []
+        for k in ks:
+            ready_tiles = back_copies[k][: len(tiles) - held] if k > 1 else None
+            targets.append(((answers if k else returned).at[k], ready_tiles))
+        narrow_group(0, targets)
+        if 1 in ks:
+            back_copies[1][0].start()
+
+    def split(sources_in, gates, ups, downs, store):
+        for i, (source, _) in enumerate(sources_in):
+            norm(source, i * slots)
+        shares_in = [share for _, share in sources_in]
         for side in range(halves):
-            widen(
-                base, [peer_scales.at[j], scales_in.at[k]], member,
-                own_gate.at[side], own_up.at[side], side,
-            )
-        blocks = [own_down.at[side] for side in range(halves)]
+            widen(0, shares_in, member, gates.at[side], ups.at[side], side)
+        blocks = [downs.at[side] for side in range(halves)]
         for column in range(len(tiles)):
-            window, total = narrow(base, 2 * slots, blocks, column)
+            window, total = narrow(0, slots * len(sources_in), blocks, column)
+            store(column, window, total)
+
+    def paired(j):
+        def store(column, window, total):
             parts_out[j, :, window] = total[:slots].astype(jnp.bfloat16)
-            half_copies[j][column].start()
-            partial[j, :, window] = total[slots:]
-
-    def joined(j, column, target, copies=None):
-        half_copies[j][column].wait_recv()
+            if j == 2:
+                half_copies[j][column].start()
+            partial[j - 1, :, window] = total[slots:]
+
+        return store
+
+    def joined(j, column, target):
         window = tiles[column]
         target[:, window] = (
-            partial[j, :, window] + parts_in[j, :, window].astype(jnp.float32)
+            partial[j - 1, :, window] + parts_in[j, :, window].astype(jnp.float32)
         ).astype(jnp.bfloat16)
-        if copies:
-            copies[column].start()
 
     def unpack(k, window):
         return lax.dot_general(
@@ -388,14 +428,21 @@
             summed[:, window] = value if fresh else summed[:, window] + value
 
     def back(k):
-        for t, window in enumerate(tiles):
-            back_copies[k][t].wait_recv()
-            summed[:, window] = summed[:, window] + unpack(k, window)
+        land(back_copies[k])
+        add(k)
 
     def finish(k):
         for t, window in enumerate(tiles):
             back_copies[k][t].wait_recv()
             out[:, window] = (summed[:, window] + unpack(k, window)).astype(jnp.bfloat16)
+
+    def flows(buffer, begin, count, sem):
+        held = buffer.at[begin : begin + count]
+        return remote(held, held, sem, back_r.at[0], twin)
+
+    def marks(count, sem):
+        held = scales.at[0:count, :members]
+        return remote(held, held, sem, back_r.at[0], twin)
 
     @on_outer
     def _():
@@ -406,95 +453,103 @@
             if i:
                 part_copies[i - 1].wait_recv()
                 far_copies[i - 1].start()
+            if i == LATE:
+                send(3)
         part_copies[-1].wait_recv()
         far_copies[-1].start()
         for copy in group_copies:
             copy.wait()
-        land(group_twins + near_copies + far_copies)
+        land(block_waits(2))
+        if FIRST:
+            arrive(3)
+            whole((3,), HELD)
         arrive(1)
-        whole((1, 0), 2 * slots)
-        send(3)
+        whole((1, 0))
         add(0, True)
+        if not FIRST:
+            arrive(3)
+            whole((3,), HELD)
         arrive(2)
-        whole((2,), 0)
-        arrive(3)
-        whole((3,), slots)
+        start(back_copies[3][len(tiles) - HELD :])
+        whole((2,))
         back(1)
-        back(3)
-        finish(2)
-        leave(peer_copies + group_twins + row_copies[3] + [scale_copies[3]] + back_copies[3])
+        half_copies[0][0].wait_recv()
+        for window in tiles:
+            summed[:, window] = summed[:, window] + lax.dot_general(
+                place[slots : 2 * slots, :], parts_in[0, :, window],
+                (((0,), (0,)), ((), ())), preferred_element_type=jnp.float32,
+            )
+        back(2)
+        finish(3)
+        leave([flows(sent, 0, 4, row_s), marks(4, scale_s), flows(answers, 1, 3, back_s)])
 
     @on_inner
     def _():
-        def take(i):
-            guest_copies[i].wait_recv()
-            cross_copies[i].start()
-            gnear_copies[i].start()
-
-        scale_copies[1].wait_recv()
-        note_copies[0].start()
-        for i in range(GROUPS):
-            row_copies[1][i].wait_recv()
-            swap_copies[0][i].start()
-            take(i)
-        relay_copies[0].start()
-        take(GROUPS)
+        def take(begin, end):
+            for i in range(begin, end):
+                guest_copies[i].wait_recv()
+                cross_copies[i].start()
+                gnear_copies[i].start()
+                if i:
+                    cross_copies[i - 1].wait_recv()
+                    gfar_copies[i - 1].start()
+
+        own = own_stores
+
+        def store_near(column, window, total):
+            answers[1, :, window] = total.astype(jnp.bfloat16)
+
+        def store_slant(column, window, total):
+            parts_out[0, :, window] = total.astype(jnp.bfloat16)
+
+        take(0, 3)
         for copy in own_copies:
             copy.wait()
-        land(own_twins + swap_copies[0] + note_copies[:1])
-        divided(0, 1)
-        start(relay_copies[1 : GROUPS + 1])
-        for i in range(GROUPS + 1, count):
-            take(i)
-            relay_copies[i].start()
-            column = i - GROUPS - 1
-            if column < GROUPS:
-                joined(0, column, answers.at[1], back_copies[1])
-            if i == SWAP_AT:
-                note_copies[1].start()
-                start(swap_copies[1])
+        land(own_twins)
+        arrive(1)
+        split([(taken.at[1], scales_in.at[1])], *own, store_near)
+        back_copies[1][0].start()
+        take(3, 4)
+        land([note_copies[1], swap_copies[1]])
+        split([(extra.at[1], extra_scales.at[1]), (taken.at[0], scales_in.at[0])], *own, paired(1))
+        swap(3)
+        half_copies[1][0].start()
+        take(4, 7)
+        land([slant_scales, slant_rows])
+        split([(extra.at[0], extra_scales.at[0])], *own, store_slant)
+        half_copies[0][0].start()
+        take(7, 10)
         arrive(2)
-        shares_in = [scales_in.at[2], scales.at[3]]
-        norm(taken.at[2], 0)
-        norm(sent.at[3], slots)
-        for i in range(count):
-            peer_copies[i].wait_recv()
-            part_copies[i].start()
-            near_copies[i].start()
-            cross_copies[i].wait_recv()
-            gfar_copies[i].start()
-            if i:
-                part_copies[i - 1].wait_recv()
-                far_copies[i - 1].start()
-            if i == wide:
-                land(gnear_copies[:wide] + gfar_copies[:wide])
-            if i == wide + members:
-                land(near_copies[:wide] + far_copies[:wide])
-            if i >= wide:
-                owner, side = (i - wide) // halves, (i - wide) % halves
-                widen_group(0, shares_in, (member + owner) % members, side)
-        part_copies[-1].wait_recv()
-        far_copies[-1].start()
-        land(
-            gnear_copies[wide:] + gfar_copies[wide:] + near_copies[wide:] + far_copies[wide:]
-        )
-        narrow_group(0, [(answers.at[2], back_copies[2]), (returned.at[3], None)])
-        land(swap_copies[1] + note_copies[1:])
-        divided(1, 0)
-        add(3, True)
+        swap(2)
+        half_copies[1][1].start()
+        take(10, count)
+        cross_copies[-1].wait_recv()
+        gfar_copies[-1].start()
+        land(block_waits(1))
+        far = [store.at[pl.ds(member * halves, halves)] for store in stores]
+        land([note_copies[2], swap_copies[2]])
+        split([(extra.at[2], extra_scales.at[2]), (taken.at[2], scales_in.at[2])], *far, paired(2))
+        land([note_copies[3], swap_copies[3]])
+        split([(extra.at[3], extra_scales.at[3]), (sent.at[3], scales.at[3])], *far, paired(3))
+        half_copies[3][0].start()
+        for column in range(len(tiles)):
+            half_copies[2][column].wait_recv()
+            joined(2, column, answers.at[2])
+            back_copies[2][column].start()
+        land(half_copies[1])
+        for column in range(len(tiles)):
+            joined(1, column, returned.at[0])
+        add(0, True)
         back(1)
-        back(2)
-        for column, window in enumerate(tiles):
-            joined(1, column, returned.at[0])
-            out[:, window] = (summed[:, window] + unpack(0, window)).astype(jnp.bfloat16)
-        leave(guest_copies + cross_copies + gnear_copies + gfar_copies + relay_copies)
-        leave(own_twins + note_copies)
-        for j in range(2):
-            leave(swap_copies[j] + half_copies[j])
-
-    leave(part_copies + near_copies + far_copies)
-    for k in (1, 2):
-        leave(row_copies[k] + [scale_copies[k]] + back_copies[k])
+        land(half_copies[3])
+        for column in range(len(tiles)):
+            joined(3, column, returned.at[3])
+        add(3)
+        finish(2)
+        leave([flows(sent, 0, 2, row_s), marks(2, scale_s), flows(answers, 1, 2, back_s)])
+        leave([flows(sent, 0, 3, swap_s), marks(3, note_s), flows(parts_out, 0, 4, half_s)])
+
+    leave(block_waits(3))
 
 
 def group_layer(members, tokens, norm_gain, route_ids, route_weights, w_gate, w_up, w_down):
@@ -535,20 +590,15 @@
             vmem(halves, features, width),
             vmem(halves, features, width),
             vmem(halves, width, features),
-            vmem(2, slots, features),
-            vmem(2, 8, slots, dtype=f32),
-            vmem(2, slots, features, dtype=f32),
-            vmem(2, slots, features),
-            vmem(2, slots, features),
-            dma, dma((3,)), dma((3,)), dma((3,)), dma((3,)),
-        ]
-        + [dma((copies,)) for _ in range(16)]
-        + [dma((GROUPS * GROUPS,)) for _ in range(2)]
-        + [dma((GROUPS,)) for _ in range(2)]
-        + [dma((GROUPS * GROUPS,)) for _ in range(2)]
-        + [dma((2 * GROUPS,)) for _ in range(2)]
-        + [dma((2,)) for _ in range(2)]
-        + [dma((2 * GROUPS,)) for _ in range(2)],
+            vmem(GROUPS, slots, features),
+            vmem(GROUPS, 8, slots, dtype=f32),
+            vmem(3, slots, features, dtype=f32),
+            vmem(GROUPS, slots, features),
+            vmem(GROUPS, slots, features),
+            dma, dma((3,)), dma((copies,)), dma((copies,)), dma((3,)), dma((3,)), dma((3,)),
+            dma, dma, dma, dma, dma, dma, dma((3,)), dma((4,)), dma((3,)), dma((4,)),
+            dma((9,)), dma((8,)),
+        ],
         compiler_params=pltpu.CompilerParams(
             collective_id=0, has_side_effects=True, vmem_limit_bytes=64400 * 1024
         ),

time: 113 us -> 93.5 us (0.83)
  the two profiles are of different devices: /device:TPU:0 before, /device:TPU:8 now
where the time goes in v5:
time: 93.5 us; the launch traced here: 92.8 us
  Pallas kernels  91.8 us (98%)
  local copies, waits for them, and re-layouts  0.97 us (1%)
    pallas_call x1, Pallas kernels, group_layer(): pl.pallas_call(functools.partial(group_kernel, members, parts, halves), o...  91.8 us

profile of v5, /device:TPU:8, one launch (start us, length us, event | category | flops | bytes accessed | tf_op | source)
XLA Modules:
  0.0 92.8 jit_solution(8602219417635726464)
XLA Ops:
  0.0 91.8 %shard_map.73 = bf16[256,2048]{1,0:T(8,128)(2,1)S(1)} custom-call(bf16[256,2048]{1,0:T(8,128)(2,1)} %tokens.1, f32[1,2048]{1,0:T(1,128)} %bitcast.9, s32[2,256]{1,0:T(2,128)} %bitcast.10, f32[2,256]{1,0:T(2,128)} %bitcast.11, bf16[2048,256]{1,0:T(8,128)(2,1)} %bitcast.6, bf16[2048,256]{1,0:T(8,128)(2,1)} %bitcast.7, bf16[256,2048]{1,0:T(8,128)(2,1)} %bitcast.8), custom_call_target="tpu_custom_call" | custom-call | tf_op jit(solution)/shard_map/pallas_call | solution.py:567
  91.8 1.0 %copy.9 = bf16[256,2048]{1,0:T(8,128)(2,1)} copy(bf16[256,2048]{1,0:T(8,128)(2,1)S(1)} %shard_map.73) | data formatting | bytes 2097152

commit v6 on v5

--- a/solution.py
+++ b/solution.py
@@ -295,13 +295,16 @@
     def _():
         start(guest_copies)
 
+    @on_outer
+    def _():
+        start(peer_copies)
+
     send(1)
 
     @on_outer
     def _():
         slant_scales.start()
         slant_rows.start()
-        start(peer_copies)
 
     pack(0)
 
@@ -479,8 +482,14 @@
                 place[slots : 2 * slots, :], parts_in[0, :, window],
                 (((0,), (0,)), ((), ())), preferred_element_type=jnp.float32,
             )
-        back(2)
-        finish(3)
+        for t, window in enumerate(tiles):
+            land([back_copies[3][t], back_copies[2][t]])
+            pair = returned[2:4, :, window].reshape(2 * slots, tile)
+            total = summed[:, window] + lax.dot_general(
+                place[2 * slots : 4 * slots, :], pair,
+                (((0,), (0,)), ((), ())), preferred_element_type=jnp.float32,
+            )
+            out[:, window] = total.astype(jnp.bfloat16)
         leave([flows(sent, 0, 4, row_s), marks(4, scale_s), flows(answers, 1, 3, back_s)])
 
     @on_inner

time: 93.5 us -> 93.4 us (level)
  no operation moved by 1% of the time
where the time goes in v6:
time: 93.4 us; the launch traced here: 92.6 us
  Pallas kernels  91.7 us (98%)
  local copies, waits for them, and re-layouts  0.97 us (1%)
    pallas_call x1, Pallas kernels, group_layer(): pl.pallas_call(functools.partial(group_kernel, members, parts, halves), o...  91.7 us

profile of v6, /device:TPU:8, one launch (start us, length us, event | category | flops | bytes accessed | tf_op | source)
XLA Modules:
  0.0 92.6 jit_solution(7169607041724159255)
XLA Ops:
  0.0 91.7 %shard_map.73 = bf16[256,2048]{1,0:T(8,128)(2,1)S(1)} custom-call(bf16[256,2048]{1,0:T(8,128)(2,1)} %tokens.1, f32[1,2048]{1,0:T(1,128)} %bitcast.9, s32[2,256]{1,0:T(2,128)} %bitcast.10, f32[2,256]{1,0:T(2,128)} %bitcast.11, bf16[2048,256]{1,0:T(8,128)(2,1)} %bitcast.6, bf16[2048,256]{1,0:T(8,128)(2,1)} %bitcast.7, bf16[256,2048]{1,0:T(8,128)(2,1)} %bitcast.8), custom_call_target="tpu_custom_call" | custom-call | tf_op jit(solution)/shard_map/pallas_call | solution.py:576
  91.7 1.0 %copy.9 = bf16[256,2048]{1,0:T(8,128)(2,1)} copy(bf16[256,2048]{1,0:T(8,128)(2,1)S(1)} %shard_map.73) | data formatting | bytes 2097152

commit v7 on v6

--- a/solution.py
+++ b/solution.py
@@ -9,9 +9,7 @@
 
 GROUPS = 4
 SPLIT = 4
-HELD = 0
 LATE = 7
-FIRST = True
 MESH = pl.DeviceIdType.MESH
 
 
@@ -379,17 +377,15 @@
                 if copies and column < len(copies):
                     copies[column].start()
 
-    def whole(ks, held=0):
-        for j, k in enumerate(ks):
-            norm(taken.at[k], j * slots)
+    def whole(ks, base=0):
         for owner in range(members):
             for side in range(halves):
-                widen_group(0, [scales_in.at[k] for k in ks], owner, side)
+                widen_group(base, [scales_in.at[k] for k in ks], owner, side)
         targets = []
         for k in ks:
-            ready_tiles = back_copies[k][: len(tiles) - held] if k > 1 else None
+            ready_tiles = back_copies[k] if k > 1 else None
             targets.append(((answers if k else returned).at[k], ready_tiles))
-        narrow_group(0, targets)
+        narrow_group(base, targets)
         if 1 in ks:
             back_copies[1][0].start()
 
@@ -458,22 +454,21 @@
                 far_copies[i - 1].start()
             if i == LATE:
                 send(3)
+        arrive(1)
+        norm(taken.at[1], 0)
+        norm(taken.at[0], slots)
+        arrive(3)
+        norm(taken.at[3], 2 * slots)
         part_copies[-1].wait_recv()
         far_copies[-1].start()
         for copy in group_copies:
             copy.wait()
         land(block_waits(2))
-        if FIRST:
-            arrive(3)
-            whole((3,), HELD)
-        arrive(1)
+        whole((3,), 2 * slots)
         whole((1, 0))
         add(0, True)
-        if not FIRST:
-            arrive(3)
-            whole((3,), HELD)
         arrive(2)
-        start(back_copies[3][len(tiles) - HELD :])
+        norm(taken.at[2], 0)
         whole((2,))
         back(1)
         half_copies[0][0].wait_recv()

time: 93.4 us -> 93 us (level)
  no operation moved by 1% of the time
where the time goes in v7:
time: 93 us; the launch traced here: 92.1 us
  Pallas kernels  91.1 us (98%)
  local copies, waits for them, and re-layouts  0.97 us (1%)
    pallas_call x1, Pallas kernels, group_layer(): pl.pallas_call(functools.partial(group_kernel, members, parts, halves), o...  91.1 us

profile of v7, /device:TPU:8, one launch (start us, length us, event | category | flops | bytes accessed | tf_op | source)
XLA Modules:
  0.0 92.1 jit_solution(14330365829778693546)
XLA Ops:
  0.0 91.1 %shard_map.73 = bf16[256,2048]{1,0:T(8,128)(2,1)S(1)} custom-call(bf16[256,2048]{1,0:T(8,128)(2,1)} %tokens.1, f32[1,2048]{1,0:T(1,128)} %bitcast.9, s32[2,256]{1,0:T(2,128)} %bitcast.10, f32[2,256]{1,0:T(2,128)} %bitcast.11, bf16[2048,256]{1,0:T(8,128)(2,1)} %bitcast.6, bf16[2048,256]{1,0:T(8,128)(2,1)} %bitcast.7, bf16[256,2048]{1,0:T(8,128)(2,1)} %bitcast.8), custom_call_target="tpu_custom_call" | custom-call | tf_op jit(solution)/shard_map/pallas_call | solution.py:571
  91.1 1.0 %copy.9 = bf16[256,2048]{1,0:T(8,128)(2,1)} copy(bf16[256,2048]{1,0:T(8,128)(2,1)S(1)} %shard_map.73) | data formatting | bytes 2097152
